TPU v7x, 128 devices: a whole 4x4x4 slice. The times are simulated.
128 devices in a mesh: sp: 32 (over z, y, core), tp: 4 (over x).
Axes of the slice: x: 4, y: 4, z: 4, core: 2. Of those that a mesh axis runs over, the one named last changes fastest.
Arguments:
- tokens: bfloat16 [12288, 4096], P(('sp', 'tp')), may hold values from -10 to 10
- norm_gain: float32 [4096], replicated, may hold values from 0.1 to 1.9
- query_weight: bfloat16 [4096, 2048], P(None, 'tp'), may hold values from -0.09375 to 0.09375
- key_weight: bfloat16 [4096, 2048], P(None, 'tp'), may hold values from -0.09375 to 0.09375
- value_weight: bfloat16 [4096, 2048], P(None, 'tp'), may hold values from -0.09375 to 0.09375
- gate_weight: bfloat16 [4096, 2048], P(None, 'tp'), may hold values from -0.09375 to 0.09375
- query_gain: float32 [128], replicated, may hold values from 0.1 to 1.9
- key_gain: float32 [128], replicated, may hold values from 0.1 to 1.9
- score_offset: float32 [16], P('tp'), may hold values from -12 to -4
- out_gain: float32 [2048], P('tp'), may hold values from 0.1 to 1.9
- out_weight: bfloat16 [2048, 4096], P('tp'), may hold values from -0.125 to 0.125
Outputs:
- layer_out: bfloat16 [12288, 4096], P(('sp', 'tp'))
All inputs are finite; a program needn't handle non-finite values.
Results may differ from a plain program's by a relative error of at most 0.03.
Values may be sent and summed in bfloat16 or wider, within the bound.
A program may use at most 192 MiB of HBM per device.

v0:
```python
import jax
import jax.numpy as jnp
from jax import lax
from jax.sharding import Mesh
from jax.sharding import PartitionSpec as P

QBLOCK = 128
SP = ("sp_0", "sp_1", "sp_2")
SP_TP = ("sp_0", "sp_1", "sp_2", "tp")


NORM_EPS = 1e-06


def laid_out(blocks, dim):
    blocks = jnp.moveaxis(blocks, 0, dim)
    shape = blocks.shape
    return blocks.reshape(*shape[:dim], shape[dim] * shape[dim + 1], *shape[dim + 2 :])


def work_in_pieces(value, axis, dim, work, out_dim):
    rows = value.shape[dim]
    pieces = jnp.split(value, 2, axis=dim) if rows % 2 == 0 else [value]
    leading = jnp.arange(lax.axis_size(axis)) * rows
    blocks = [lax.all_gather(piece, axis) for piece in pieces]
    made = [jax.vmap(work)(b, leading + k * (rows // len(pieces))) for k, b in enumerate(blocks)]
    return laid_out(jnp.concatenate(made, axis=out_dim + 1), out_dim)


def side_by_side(arrays, axis, dim, along):
    widths = [a.shape[along] for a in arrays]
    both = jnp.concatenate(arrays, axis=along)
    out = lax.all_gather(both, axis, axis=dim, tiled=True)
    return tuple(jnp.split(out, [sum(widths[:k]) for k in range(1, len(widths))], axis=along))


def in_blocks(value, dim, count):
    before, after = (value.shape[:dim], value.shape[dim + 1 :])
    return jnp.moveaxis(value.reshape(*before, count, -1, *after), dim, 0)


def exchange_in_order(blocks, axes, turns):
    shape = [lax.axis_size(a) for a in axes]
    blocks = blocks.reshape(*shape, *blocks.shape[1:])
    for k in turns:
        blocks = lax.all_to_all(blocks, axes[k], split_axis=k, concat_axis=k, tiled=True)
    return blocks.reshape(-1, *blocks.shape[len(axes) :])


def core_and_chips(value, groups, turns, split_dim, concat_dim):
    count = lax.axis_size(groups[0]) * lax.axis_size(groups[1])
    blocks = in_blocks(value, split_dim, count)
    return laid_out(exchange_in_order(blocks, groups, turns), concat_dim)


def sent_and_summed(value, axis, dim):
    blocks = in_blocks(value, dim, lax.axis_size(axis))
    arrived = lax.all_to_all(blocks, axis, split_axis=0, concat_axis=0, tiled=True)
    return arrived.astype(jnp.float32).sum(axis=0)


def rms_rows(inputs, gain_vec):
    inputs = inputs.astype(jnp.float32)
    scaled = inputs * lax.rsqrt(jnp.mean(inputs * inputs, axis=-1, keepdims=True) + NORM_EPS)
    return scaled * gain_vec


def on_device(
    tokens,
    norm_gain,
    query_weight,
    key_weight,
    value_weight,
    gate_weight,
    query_gain,
    key_gain,
    score_offset,
    out_gain,
    out_weight,
):
    heads_local = score_offset.shape[0]
    head_dim = query_gain.shape[0]
    width_local = query_weight.shape[1]
    normed = rms_rows(tokens, norm_gain).astype(jnp.bfloat16)
    matrices = (query_weight, key_weight, value_weight, gate_weight)

    def project(piece, first_row):
        return jnp.stack(
            [
                jnp.dot(piece, matrix, preferred_element_type=jnp.float32).astype(jnp.bfloat16)
                for matrix in matrices
            ],
            axis=1,
        )

    projected = work_in_pieces(normed, "tp", 0, project, 0)
    row_count = projected.shape[0]
    queries = (
        rms_rows(projected[:, 0].reshape(row_count, heads_local, head_dim), query_gain)
        .astype(jnp.bfloat16)
        .reshape(row_count, width_local)
    )
    key_rows = (
        rms_rows(projected[:, 1].reshape(row_count, heads_local, head_dim), key_gain)
        .astype(jnp.bfloat16)
        .reshape(row_count, width_local)
    )
    value_rows = projected[:, 2]
    gate_rows = projected[:, 3]
    shards = lax.axis_size(SP)
    own_index = lax.axis_index(SP)
    local_rows = jnp.arange(row_count, dtype=jnp.int32)
    queries = lax.all_to_all(queries, SP, split_axis=0, concat_axis=0, tiled=True)
    slice_rows = row_count // shards
    query_pos = (
        local_rows // slice_rows * row_count + own_index * slice_rows + local_rows % slice_rows
    )
    query_heads = queries.reshape(row_count, heads_local, head_dim)
    blocks = row_count // QBLOCK
    score_scale = head_dim ** (-0.5)

    def score_block(query_block, key_block, pos_block, key_pos):
        scores = jnp.einsum(
            "qhd,khd->hqk", query_block, key_block, preferred_element_type=jnp.float32
        )
        scores = scores * score_scale + score_offset[:, None, None]
        causal = key_pos[None, None, :] < pos_block[None, :, None]
        return (scores, causal)

    def query_slices(which_block):
        query_start = which_block * QBLOCK
        query_block = lax.dynamic_slice_in_dim(query_heads, query_start, QBLOCK, 0)
        pos_block = lax.dynamic_slice_in_dim(query_pos, query_start, QBLOCK, 0)
        return (query_start, query_block, pos_block)

    def stick_sums(scores, causal, carried, value_block):
        fail_log = jnp.where(causal, jax.nn.log_sigmoid(-scores), 0.0)
        later_sum = lax.cumsum(fail_log, axis=2, reverse=True) - fail_log + carried[:, :, None]
        stick = jnp.where(causal, jnp.exp(jax.nn.log_sigmoid(scores) + later_sum), 0.0).astype(
            jnp.bfloat16
        )
        sums = jnp.einsum("hqk,khd->qhd", stick, value_block, preferred_element_type=jnp.float32)
        return (sums, jnp.sum(fail_log, axis=2))

    empty_sums = jnp.zeros((row_count, heads_local, head_dim), jnp.float32)
    key_all, value_all = side_by_side((key_rows, value_rows), SP, 0, 1)
    shard_count = key_all.shape[0] // row_count

    def one_shard(step, state):
        which_shard = shard_count - 1 - step
        key_start = which_shard * row_count
        key_block = lax.dynamic_slice_in_dim(key_all, key_start, row_count, 0).reshape(
            row_count, heads_local, head_dim
        )
        value_block = lax.dynamic_slice_in_dim(value_all, key_start, row_count, 0).reshape(
            row_count, heads_local, head_dim
        )
        key_pos = key_start + local_rows

        def one_block(which_block, state):
            running, carried_all = state
            query_start, query_block, pos_block = query_slices(which_block)
            carried = lax.dynamic_slice(carried_all, (0, query_start), (heads_local, QBLOCK))

            def compute(unused):
                scores, causal = score_block(query_block, key_block, pos_block, key_pos)
                return stick_sums(scores, causal, carried, value_block)

            def skipped(unused):
                return (
                    jnp.zeros((QBLOCK, heads_local, head_dim), jnp.float32),
                    jnp.zeros((heads_local, QBLOCK), jnp.float32),
                )

            needed = key_start < jnp.max(pos_block)
            partial_value, block_total = lax.cond(needed, compute, skipped, 0)
            current = lax.dynamic_slice(
                running, (query_start, 0, 0), (QBLOCK, heads_local, head_dim)
            )
            running = lax.dynamic_update_slice(
                running, current + partial_value, (query_start, 0, 0)
            )
            carried_all = lax.dynamic_update_slice(
                carried_all, carried + block_total, (0, query_start)
            )
            return (running, carried_all)

        return lax.fori_loop(0, blocks, one_block, state)

    start_state = (empty_sums, jnp.zeros((heads_local, row_count), jnp.float32))
    attended = lax.fori_loop(0, shard_count, one_shard, start_state)[0]
    attended = attended.astype(jnp.bfloat16).reshape(row_count, width_local)
    attended = core_and_chips(attended, (("sp_0", "sp_1"), "sp_2"), (1, 0), 0, 0)
    normed_out = rms_rows(
        attended.reshape(row_count, heads_local, head_dim), out_gain.reshape(heads_local, head_dim)
    ).reshape(row_count, width_local)
    mixed_rows = (normed_out * jax.nn.silu(gate_rows.astype(jnp.float32))).astype(jnp.bfloat16)
    return sent_and_summed(
        jnp.dot(mixed_rows, out_weight, preferred_element_type=jnp.float32).astype(jnp.bfloat16),
        "tp",
        0,
    ).astype(jnp.bfloat16)


def solution(mesh):
    finer = Mesh(mesh.devices.reshape(4, 4, 2, mesh.shape["tp"]), ("sp_0", "sp_1", "sp_2", "tp"))
    in_specs = (
        P(SP_TP, None),
        P(),
        P(None, "tp"),
        P(None, "tp"),
        P(None, "tp"),
        P(None, "tp"),
        P(),
        P(),
        P("tp"),
        P("tp"),
        P("tp", None),
    )
    out_specs = P(SP_TP, None)
    return jax.shard_map(
        on_device, mesh=finer, in_specs=in_specs, out_specs=out_specs, check_vma=False
    )
```

profile of v0, /device:TPU:1, one launch (start us, length us, event | category | flops | bytes accessed | tf_op | source)
XLA Modules:
  0.0 1258.9 jit_solution(5365857525228447160)
XLA Ops:
  11.1 28.8 %all-gather.10.cloned.1.call-done = bf16[192,4096]{1,0:T(8,128)(2,1)} async-done(((bf16[48,4096]{1,0:T(8,128)(2,1)}), bf16[192,4096]{1,0:T(8,128)(2,1)}) %all-gather.10.cloned.1.call-update) | async-done | bytes 1572880 | tf_op jit(solution)/shard_map/all_gather | solution.py:25
  45.3 22.7 %all-gather.8.cloned.1.call-done = bf16[192,4096]{1,0:T(8,128)(2,1)} async-done(((bf16[48,4096]{1,0:T(8,128)(2,1)}), bf16[192,4096]{1,0:T(8,128)(2,1)}) %all-gather.8.cloned.1.call-update) | async-done | bytes 1572880 | tf_op jit(solution)/shard_map/all_gather | solution.py:25
  97.6 15.8 %all-to-all-done = bf16[32,12,512]{2,1,0:T(8,128)(2,1)S(1)} async-done(((bf16[32,12,512]{2,1,0:T(8,128)(2,1)}), bf16[32,12,512]{2,1,0:T(8,128)(2,1)S(1)}, u32[]{:S(2)}, u32[]{:S(2)}) %all-to-all-start) | async-done | bytes 393248 | tf_op jit(solution)/shard_map/all_to_all | solution.py:113
  114.4 68.7 %all-gather.6.cloned.1.call-done = bf16[12288,1024]{1,0:T(8,128)(2,1)} async-done(((bf16[384,1024]{1,0:T(8,128)(2,1)}), bf16[12288,1024]{1,0:T(8,128)(2,1)}) %all-gather.6.cloned.1.call-update) | async-done | bytes 25165840 | tf_op jit(solution)/shard_map/all_gather | solution.py:33
  183.1 16.9 %fusion.112 = (bf16[12288,512]{1,0:T(8,128)(2,1)}, bf16[12288,512]{1,0:T(8,128)(2,1)}) fusion(bf16[12288,1024]{1,0:T(8,128)(2,1)} %all-gather.6.cloned.1.call-done), kind=kLoop, calls=%fused_computation.116 | loop fusion | bytes 50331648 | tf_op jit(solution)/shard_map/split | solution.py:34
  201.0 982.9 %while.45 = (s32[]{:T(128)}, f32[384,4,128]{2,0,1:T(8,128)}, f32[4,384]{1,0:T(4,128)S(1)}, bf16[12288,512]{1,0:T(8,128)(2,1)}, bf16[12288,512]{1,0:T(8,128)(2,1)...) while((s32[]{:T(128)}, f32[384,4,128]{2,0,1:T(8,128)}, ...), condition=%wide.region_12.13_spmd.clone, body=%wide.region_3.12_spmd.clone.sunk | while | flops 134359168 | bytes 20416180 | solution.py:191
  203.7 18.4 %while.46 = (s32[]{:T(128)}, f32[384,4,128]{2,0,1:T(8,128)}, f32[4,384]{1,0:T(4,128)S(1)}, s32[384]{0:T(512)S(1)}, s32[]{:T(128)}, /*index=5*/s32[384]{0:T(512)S...) while((s32[]{:T(128)}, f32[384,4,128]{2,0,1:T(8,128)}, ...), condition=%wide.region_11.11_spmd, body=%wide.region_4.10_spmd.sunk | while | flops 134353024 | bytes 15694161 | solution.py:188
  225.0 18.4 %while.46 = (s32[]{:T(128)}, f32[384,4,128]{2,0,1:T(8,128)}, f32[4,384]{1,0:T(4,128)S(1)}, s32[384]{0:T(512)S(1)}, s32[]{:T(128)}, /*index=5*/s32[384]{0:T(512)S...) while((s32[]{:T(128)}, f32[384,4,128]{2,0,1:T(8,128)}, ...), condition=%wide.region_11.11_spmd, body=%wide.region_4.10_spmd.sunk | while | flops 134353024 | bytes 15694161 | solution.py:188
  246.2 18.4 %while.46 = (s32[]{:T(128)}, f32[384,4,128]{2,0,1:T(8,128)}, f32[4,384]{1,0:T(4,128)S(1)}, s32[384]{0:T(512)S(1)}, s32[]{:T(128)}, /*index=5*/s32[384]{0:T(512)S...) while((s32[]{:T(128)}, f32[384,4,128]{2,0,1:T(8,128)}, ...), condition=%wide.region_11.11_spmd, body=%wide.region_4.10_spmd.sunk | while | flops 134353024 | bytes 15694161 | solution.py:188
  253.6 9.3 conditional.2
  267.4 18.4 %while.46 = (s32[]{:T(128)}, f32[384,4,128]{2,0,1:T(8,128)}, f32[4,384]{1,0:T(4,128)S(1)}, s32[384]{0:T(512)S(1)}, s32[]{:T(128)}, /*index=5*/s32[384]{0:T(512)S...) while((s32[]{:T(128)}, f32[384,4,128]{2,0,1:T(8,128)}, ...), condition=%wide.region_11.11_spmd, body=%wide.region_4.10_spmd.sunk | while | flops 134353024 | bytes 15694161 | solution.py:188
  288.6 18.4 %while.46 = (s32[]{:T(128)}, f32[384,4,128]{2,0,1:T(8,128)}, f32[4,384]{1,0:T(4,128)S(1)}, s32[384]{0:T(512)S(1)}, s32[]{:T(128)}, /*index=5*/s32[384]{0:T(512)S...) while((s32[]{:T(128)}, f32[384,4,128]{2,0,1:T(8,128)}, ...), condition=%wide.region_11.11_spmd, body=%wide.region_4.10_spmd.sunk | while | flops 134353024 | bytes 15694161 | solution.py:188
  309.8 18.4 %while.46 = (s32[]{:T(128)}, f32[384,4,128]{2,0,1:T(8,128)}, f32[4,384]{1,0:T(4,128)S(1)}, s32[384]{0:T(512)S(1)}, s32[]{:T(128)}, /*index=5*/s32[384]{0:T(512)S...) while((s32[]{:T(128)}, f32[384,4,128]{2,0,1:T(8,128)}, ...), condition=%wide.region_11.11_spmd, body=%wide.region_4.10_spmd.sunk | while | flops 134353024 | bytes 15694161 | solution.py:188
  331.0 18.4 %while.46 = (s32[]{:T(128)}, f32[384,4,128]{2,0,1:T(8,128)}, f32[4,384]{1,0:T(4,128)S(1)}, s32[384]{0:T(512)S(1)}, s32[]{:T(128)}, /*index=5*/s32[384]{0:T(512)S...) while((s32[]{:T(128)}, f32[384,4,128]{2,0,1:T(8,128)}, ...), condition=%wide.region_11.11_spmd, body=%wide.region_4.10_spmd.sunk | while | flops 134353024 | bytes 15694161 | solution.py:188
  338.4 9.3 conditional.2
  352.2 18.4 %while.46 = (s32[]{:T(128)}, f32[384,4,128]{2,0,1:T(8,128)}, f32[4,384]{1,0:T(4,128)S(1)}, s32[384]{0:T(512)S(1)}, s32[]{:T(128)}, /*index=5*/s32[384]{0:T(512)S...) while((s32[]{:T(128)}, f32[384,4,128]{2,0,1:T(8,128)}, ...), condition=%wide.region_11.11_spmd, body=%wide.region_4.10_spmd.sunk | while | flops 134353024 | bytes 15694161 | solution.py:188
  373.4 18.4 %while.46 = (s32[]{:T(128)}, f32[384,4,128]{2,0,1:T(8,128)}, f32[4,384]{1,0:T(4,128)S(1)}, s32[384]{0:T(512)S(1)}, s32[]{:T(128)}, /*index=5*/s32[384]{0:T(512)S...) while((s32[]{:T(128)}, f32[384,4,128]{2,0,1:T(8,128)}, ...), condition=%wide.region_11.11_spmd, body=%wide.region_4.10_spmd.sunk | while | flops 134353024 | bytes 15694161 | solution.py:188
  380.8 9.3 conditional.2
  394.6 18.4 %while.46 = (s32[]{:T(128)}, f32[384,4,128]{2,0,1:T(8,128)}, f32[4,384]{1,0:T(4,128)S(1)}, s32[384]{0:T(512)S(1)}, s32[]{:T(128)}, /*index=5*/s32[384]{0:T(512)S...) while((s32[]{:T(128)}, f32[384,4,128]{2,0,1:T(8,128)}, ...), condition=%wide.region_11.11_spmd, body=%wide.region_4.10_spmd.sunk | while | flops 134353024 | bytes 15694161 | solution.py:188
  415.8 27.6 %while.46 = (s32[]{:T(128)}, f32[384,4,128]{2,0,1:T(8,128)}, f32[4,384]{1,0:T(4,128)S(1)}, s32[384]{0:T(512)S(1)}, s32[]{:T(128)}, /*index=5*/s32[384]{0:T(512)S...) while((s32[]{:T(128)}, f32[384,4,128]{2,0,1:T(8,128)}, ...), condition=%wide.region_11.11_spmd, body=%wide.region_4.10_spmd.sunk | while | flops 134353024 | bytes 15694161 | solution.py:188
  446.3 27.6 %while.46 = (s32[]{:T(128)}, f32[384,4,128]{2,0,1:T(8,128)}, f32[4,384]{1,0:T(4,128)S(1)}, s32[384]{0:T(512)S(1)}, s32[]{:T(128)}, /*index=5*/s32[384]{0:T(512)S...) while((s32[]{:T(128)}, f32[384,4,128]{2,0,1:T(8,128)}, ...), condition=%wide.region_11.11_spmd, body=%wide.region_4.10_spmd.sunk | while | flops 134353024 | bytes 15694161 | solution.py:188
  476.7 27.6 %while.46 = (s32[]{:T(128)}, f32[384,4,128]{2,0,1:T(8,128)}, f32[4,384]{1,0:T(4,128)S(1)}, s32[384]{0:T(512)S(1)}, s32[]{:T(128)}, /*index=5*/s32[384]{0:T(512)S...) while((s32[]{:T(128)}, f32[384,4,128]{2,0,1:T(8,128)}, ...), condition=%wide.region_11.11_spmd, body=%wide.region_4.10_spmd.sunk | while | flops 134353024 | bytes 15694161 | solution.py:188
  493.3 9.3 conditional.2
  507.1 27.6 %while.46 = (s32[]{:T(128)}, f32[384,4,128]{2,0,1:T(8,128)}, f32[4,384]{1,0:T(4,128)S(1)}, s32[384]{0:T(512)S(1)}, s32[]{:T(128)}, /*index=5*/s32[384]{0:T(512)S...) while((s32[]{:T(128)}, f32[384,4,128]{2,0,1:T(8,128)}, ...), condition=%wide.region_11.11_spmd, body=%wide.region_4.10_spmd.sunk | while | flops 134353024 | bytes 15694161 | solution.py:188
  537.6 27.6 %while.46 = (s32[]{:T(128)}, f32[384,4,128]{2,0,1:T(8,128)}, f32[4,384]{1,0:T(4,128)S(1)}, s32[384]{0:T(512)S(1)}, s32[]{:T(128)}, /*index=5*/s32[384]{0:T(512)S...) while((s32[]{:T(128)}, f32[384,4,128]{2,0,1:T(8,128)}, ...), condition=%wide.region_11.11_spmd, body=%wide.region_4.10_spmd.sunk | while | flops 134353024 | bytes 15694161 | solution.py:188
  568.0 27.6 %while.46 = (s32[]{:T(128)}, f32[384,4,128]{2,0,1:T(8,128)}, f32[4,384]{1,0:T(4,128)S(1)}, s32[384]{0:T(512)S(1)}, s32[]{:T(128)}, /*index=5*/s32[384]{0:T(512)S...) while((s32[]{:T(128)}, f32[384,4,128]{2,0,1:T(8,128)}, ...), condition=%wide.region_11.11_spmd, body=%wide.region_4.10_spmd.sunk | while | flops 134353024 | bytes 15694161 | solution.py:188
  598.4 27.6 %while.46 = (s32[]{:T(128)}, f32[384,4,128]{2,0,1:T(8,128)}, f32[4,384]{1,0:T(4,128)S(1)}, s32[384]{0:T(512)S(1)}, s32[]{:T(128)}, /*index=5*/s32[384]{0:T(512)S...) while((s32[]{:T(128)}, f32[384,4,128]{2,0,1:T(8,128)}, ...), condition=%wide.region_11.11_spmd, body=%wide.region_4.10_spmd.sunk | while | flops 134353024 | bytes 15694161 | solution.py:188
  615.0 9.3 conditional.2
  628.8 27.6 %while.46 = (s32[]{:T(128)}, f32[384,4,128]{2,0,1:T(8,128)}, f32[4,384]{1,0:T(4,128)S(1)}, s32[384]{0:T(512)S(1)}, s32[]{:T(128)}, /*index=5*/s32[384]{0:T(512)S...) while((s32[]{:T(128)}, f32[384,4,128]{2,0,1:T(8,128)}, ...), condition=%wide.region_11.11_spmd, body=%wide.region_4.10_spmd.sunk | while | flops 134353024 | bytes 15694161 | solution.py:188
  659.3 27.6 %while.46 = (s32[]{:T(128)}, f32[384,4,128]{2,0,1:T(8,128)}, f32[4,384]{1,0:T(4,128)S(1)}, s32[384]{0:T(512)S(1)}, s32[]{:T(128)}, /*index=5*/s32[384]{0:T(512)S...) while((s32[]{:T(128)}, f32[384,4,128]{2,0,1:T(8,128)}, ...), condition=%wide.region_11.11_spmd, body=%wide.region_4.10_spmd.sunk | while | flops 134353024 | bytes 15694161 | solution.py:188
  689.7 27.6 %while.46 = (s32[]{:T(128)}, f32[384,4,128]{2,0,1:T(8,128)}, f32[4,384]{1,0:T(4,128)S(1)}, s32[384]{0:T(512)S(1)}, s32[]{:T(128)}, /*index=5*/s32[384]{0:T(512)S...) while((s32[]{:T(128)}, f32[384,4,128]{2,0,1:T(8,128)}, ...), condition=%wide.region_11.11_spmd, body=%wide.region_4.10_spmd.sunk | while | flops 134353024 | bytes 15694161 | solution.py:188
  720.1 27.6 %while.46 = (s32[]{:T(128)}, f32[384,4,128]{2,0,1:T(8,128)}, f32[4,384]{1,0:T(4,128)S(1)}, s32[384]{0:T(512)S(1)}, s32[]{:T(128)}, /*index=5*/s32[384]{0:T(512)S...) while((s32[]{:T(128)}, f32[384,4,128]{2,0,1:T(8,128)}, ...), condition=%wide.region_11.11_spmd, body=%wide.region_4.10_spmd.sunk | while | flops 134353024 | bytes 15694161 | solution.py:188
  736.8 9.3 conditional.2
  750.5 36.9 %while.46 = (s32[]{:T(128)}, f32[384,4,128]{2,0,1:T(8,128)}, f32[4,384]{1,0:T(4,128)S(1)}, s32[384]{0:T(512)S(1)}, s32[]{:T(128)}, /*index=5*/s32[384]{0:T(512)S...) while((s32[]{:T(128)}, f32[384,4,128]{2,0,1:T(8,128)}, ...), condition=%wide.region_11.11_spmd, body=%wide.region_4.10_spmd.sunk | while | flops 134353024 | bytes 15694161 | solution.py:188
  764.1 9.3 conditional.2
  790.2 36.9 %while.46 = (s32[]{:T(128)}, f32[384,4,128]{2,0,1:T(8,128)}, f32[4,384]{1,0:T(4,128)S(1)}, s32[384]{0:T(512)S(1)}, s32[]{:T(128)}, /*index=5*/s32[384]{0:T(512)S...) while((s32[]{:T(128)}, f32[384,4,128]{2,0,1:T(8,128)}, ...), condition=%wide.region_11.11_spmd, body=%wide.region_4.10_spmd.sunk | while | flops 134353024 | bytes 15694161 | solution.py:188
  791.5 9.3 conditional.2
  829.8 36.9 %while.46 = (s32[]{:T(128)}, f32[384,4,128]{2,0,1:T(8,128)}, f32[4,384]{1,0:T(4,128)S(1)}, s32[384]{0:T(512)S(1)}, s32[]{:T(128)}, /*index=5*/s32[384]{0:T(512)S...) while((s32[]{:T(128)}, f32[384,4,128]{2,0,1:T(8,128)}, ...), condition=%wide.region_11.11_spmd, body=%wide.region_4.10_spmd.sunk | while | flops 134353024 | bytes 15694161 | solution.py:188
  869.5 36.9 %while.46 = (s32[]{:T(128)}, f32[384,4,128]{2,0,1:T(8,128)}, f32[4,384]{1,0:T(4,128)S(1)}, s32[384]{0:T(512)S(1)}, s32[]{:T(128)}, /*index=5*/s32[384]{0:T(512)S...) while((s32[]{:T(128)}, f32[384,4,128]{2,0,1:T(8,128)}, ...), condition=%wide.region_11.11_spmd, body=%wide.region_4.10_spmd.sunk | while | flops 134353024 | bytes 15694161 | solution.py:188
  909.1 36.9 %while.46 = (s32[]{:T(128)}, f32[384,4,128]{2,0,1:T(8,128)}, f32[4,384]{1,0:T(4,128)S(1)}, s32[384]{0:T(512)S(1)}, s32[]{:T(128)}, /*index=5*/s32[384]{0:T(512)S...) while((s32[]{:T(128)}, f32[384,4,128]{2,0,1:T(8,128)}, ...), condition=%wide.region_11.11_spmd, body=%wide.region_4.10_spmd.sunk | while | flops 134353024 | bytes 15694161 | solution.py:188
  948.8 36.9 %while.46 = (s32[]{:T(128)}, f32[384,4,128]{2,0,1:T(8,128)}, f32[4,384]{1,0:T(4,128)S(1)}, s32[384]{0:T(512)S(1)}, s32[]{:T(128)}, /*index=5*/s32[384]{0:T(512)S...) while((s32[]{:T(128)}, f32[384,4,128]{2,0,1:T(8,128)}, ...), condition=%wide.region_11.11_spmd, body=%wide.region_4.10_spmd.sunk | while | flops 134353024 | bytes 15694161 | solution.py:188
  988.4 36.9 %while.46 = (s32[]{:T(128)}, f32[384,4,128]{2,0,1:T(8,128)}, f32[4,384]{1,0:T(4,128)S(1)}, s32[384]{0:T(512)S(1)}, s32[]{:T(128)}, /*index=5*/s32[384]{0:T(512)S...) while((s32[]{:T(128)}, f32[384,4,128]{2,0,1:T(8,128)}, ...), condition=%wide.region_11.11_spmd, body=%wide.region_4.10_spmd.sunk | while | flops 134353024 | bytes 15694161 | solution.py:188
  1028.1 36.9 %while.46 = (s32[]{:T(128)}, f32[384,4,128]{2,0,1:T(8,128)}, f32[4,384]{1,0:T(4,128)S(1)}, s32[384]{0:T(512)S(1)}, s32[]{:T(128)}, /*index=5*/s32[384]{0:T(512)S...) while((s32[]{:T(128)}, f32[384,4,128]{2,0,1:T(8,128)}, ...), condition=%wide.region_11.11_spmd, body=%wide.region_4.10_spmd.sunk | while | flops 134353024 | bytes 15694161 | solution.py:188
  1067.7 36.9 %while.46 = (s32[]{:T(128)}, f32[384,4,128]{2,0,1:T(8,128)}, f32[4,384]{1,0:T(4,128)S(1)}, s32[384]{0:T(512)S(1)}, s32[]{:T(128)}, /*index=5*/s32[384]{0:T(512)S...) while((s32[]{:T(128)}, f32[384,4,128]{2,0,1:T(8,128)}, ...), condition=%wide.region_11.11_spmd, body=%wide.region_4.10_spmd.sunk | while | flops 134353024 | bytes 15694161 | solution.py:188
  1107.4 36.9 %while.46 = (s32[]{:T(128)}, f32[384,4,128]{2,0,1:T(8,128)}, f32[4,384]{1,0:T(4,128)S(1)}, s32[384]{0:T(512)S(1)}, s32[]{:T(128)}, /*index=5*/s32[384]{0:T(512)S...) while((s32[]{:T(128)}, f32[384,4,128]{2,0,1:T(8,128)}, ...), condition=%wide.region_11.11_spmd, body=%wide.region_4.10_spmd.sunk | while | flops 134353024 | bytes 15694161 | solution.py:188
  1147.0 36.9 %while.46 = (s32[]{:T(128)}, f32[384,4,128]{2,0,1:T(8,128)}, f32[4,384]{1,0:T(4,128)S(1)}, s32[384]{0:T(512)S(1)}, s32[]{:T(128)}, /*index=5*/s32[384]{0:T(512)S...) while((s32[]{:T(128)}, f32[384,4,128]{2,0,1:T(8,128)}, ...), condition=%wide.region_11.11_spmd, body=%wide.region_4.10_spmd.sunk | while | flops 134353024 | bytes 15694161 | solution.py:188
  1190.2 14.0 %all_to_all.22 = bf16[16,2,12,512]{3,1,2,0:T(2,128)(2,1)S(1)} all-to-all(bf16[16,2,12,512]{3,1,2,0:T(2,128)(2,1)S(1)} %copy.71), channel_id=1, replica_groups=mesh['sp_0'=4,'sp_1'=4,'sp_2'=2,'tp'=4] {'sp_0','sp_1'}, dimensions={0} | all-to-all | bytes 786432 | tf_op jit(solution)/shard_map/all_to_all | solution.py:46
  1211.1 39.6 %all_to_all.23 = bf16[4,96,4096]{2,1,0:T(8,128)(2,1)S(1)} all-to-all(bf16[4,96,4096]{2,1,0:T(8,128)(2,1)S(1)} %bitcast.142), channel_id=1, replica_groups=mesh['sp_0'=4,'sp_1'=4,'sp_2'=2,'tp'=4] {'tp'}, dimensions={0} | all-to-all | bytes 6291456 | tf_op jit(solution)/shard_map/all_to_all | solution.py:58
  (1720 shorter events, 1506.0 us)
Async XLA Ops:
  6.5 4.6 copy-start
  6.5 33.4 %all-gather.10.cloned.1.call-start = ((), (), s32[]{:S(2)}) async-start(), calls=%async_computation.6 | async-start | bytes 1966080 | tf_op jit(solution)/shard_map/all_gather | solution.py:25
  10.3 57.7 %all-gather.8.cloned.1.call-start = ((), (), s32[]{:S(2)}) async-start(), calls=%async_computation.5 | async-start | bytes 1966080 | tf_op jit(solution)/shard_map/all_gather | solution.py:25
  11.1 172.0 %all-gather.6.cloned.1.call-start = ((), (), s32[]{:S(2)}) async-start(), calls=%async_computation.4 | async-start | bytes 25952256 | tf_op jit(solution)/shard_map/all_gather | solution.py:33
  39.9 3.9 copy-start.7
  39.9 4.4 copy-start.11
  68.0 3.9 copy-start.8
  68.0 4.4 copy-start.12
  72.4 2.2 copy-start.9
  75.6 2.2 copy-start.10
  80.0 5.7 copy-start.3
  83.1 3.9 copy-start.6
  85.2 1.8 copy-start.4
  89.7 23.7 %all-to-all-start = ((bf16[32,12,512]{2,1,0:T(8,128)(2,1)}), bf16[32,12,512]{2,1,0:T(8,128)(2,1)S(1)}, u32[]{:S(2)}, u32[]{:S(2)}) async-start(bf16[32,12,512]{2,1,0:T(8,128)(2,1)} %multiply_convert_fusion), calls=%async_computation | async-start | bytes 1048576 | tf_op jit(solution)/shard_map/all_to_all | solution.py:113
  114.4 86.6 %copy-start.5 = (f32[4]{0:T(128)S(1)}, f32[4]{0:T(128)}, u32[]{:S(2)}) copy-start(f32[4]{0:T(128)} %param.25) | copy-start | bytes 52
  218.1 1.0 copy-start.2
  239.3 1.0 copy-start.2
  260.5 1.0 copy-start.2
  281.7 1.0 copy-start.2
  302.9 1.0 copy-start.2
  324.2 1.0 copy-start.2
  345.4 1.0 copy-start.2
  366.6 1.0 copy-start.2
  387.8 1.0 copy-start.2
  409.0 1.0 copy-start.2
  427.1 1.0 copy-start.2
  439.4 1.0 copy-start.2
  457.6 1.0 copy-start.2
  469.9 1.0 copy-start.2
  488.0 1.0 copy-start.2
  500.3 1.0 copy-start.2
  518.4 1.0 copy-start.2
  530.7 1.0 copy-start.2
  548.9 1.0 copy-start.2
  561.1 1.0 copy-start.2
  579.3 1.0 copy-start.2
  591.6 1.0 copy-start.2
  609.7 1.0 copy-start.2
  622.0 1.0 copy-start.2
  640.1 1.0 copy-start.2
  652.4 1.0 copy-start.2
  670.6 1.0 copy-start.2
  682.9 1.0 copy-start.2
  877.7 1.0 copy-start.2
  1088.2 1.0 copy-start.2
  1100.5 1.0 copy-start.2
  1205.6 1.2 copy-start.13
  1211.1 41.3 %copy-start.1 = (f32[128]{0:T(128)S(1)}, f32[128]{0:T(128)}, u32[]{:S(2)}) copy-start(f32[128]{0:T(128)} %param.24) | copy-start | bytes 1540
  (34 other events, 33.9 us)
Sparse Core Ops, SparseCore 0:
  10.4 29.4 all-gather.9
  41.6 26.4 all-gather.7
  87.1 96.0 all-gather.5
where the time goes:
time: 1270 us; the launch traced here: 1260 us
  other arithmetic  610 us (48%)
  matrix products  187 us (15%)
  local copies, waits for them, and re-layouts  183 us (14%)
  waiting for transfers between devices  137 us (11%)
  loops' own time  63.6 us (5%)
  blocking collectives  57.7 us (5%)
  between operations  13.5 us (1%)
    another operation x130, other arithmetic  305 us
    dynamic_update_slice x96, other arithmetic, one_block(): lax.dynamic_update_slice(running, current + partial_value, (query_start,...  164 us
    dot_general x65, matrix products, stick_sums(): jnp.einsum('hqk,khd->qhd', stick, value_block, preferred_element_type=jnp...  87.1 us
    dot_general x65, matrix products, score_block(): jnp.einsum('qhd,khd->hqk', query_block, key_block, preferred_element_type...  81.9 us
    all_gather x1, waiting for transfers between devices, side_by_side(): out = lax.all_gather(both, axis, axis=dim, tiled=True)  68.7 us
    reduce_max x96, other arithmetic, one_block(): needed = key_start < jnp.max(pos_block)  66.7 us
    another operation x32, loops' own time, one_shard(): return lax.fori_loop(0, blocks, one_block, state)  55.8 us
    all_gather x2, waiting for transfers between devices, work_in_pieces(): blocks = [lax.all_gather(piece, axis) for piece in pieces]  51.5 us
  transfers between devices with their start and end apart: 4, of which 4 were waited for; matrix products, arithmetic and copies ran while one was open for 1% of the time, Pallas kernels for 0%

commit v1 on v0

v1 whole, which is shorter than its diff:
```python
import functools

import jax
import jax.numpy as jnp
from jax import lax
from jax.experimental import pallas as pl
from jax.experimental.pallas import tpu as pltpu
from jax.sharding import Mesh
from jax.sharding import PartitionSpec as P

SP = ("sp_0", "sp_1", "sp_2")
SP_TP = ("sp_0", "sp_1", "sp_2", "tp")
NORM_EPS = 1e-06

NQ = 384
KS = 512
KP = 256
LOG2E = 1.4426950408889634

def attention_kernel(blocks_of, q_ref, off_ref, ka_ref, kb_ref, va_ref, vb_ref, tri_ref, o_ref, acc_ref, carry_ref):
    off = off_ref[0]
    blks = blocks_of()
    for i in range(4):
        b = blks[i]
        acc_ref[...] = jnp.zeros_like(acc_ref)
        carry_ref[...] = jnp.zeros_like(carry_ref)
        n_hi = (b * NQ + NQ + KS - 1) // KS
        n_lo = (b * NQ) // KS
        def step(k, masked, i=i, b=b):
            start = pl.multiple_of(k * KP, KP)
            q = q_ref[i]
            ka = ka_ref[pl.ds(start, KP), :]
            kb = kb_ref[pl.ds(start, KP), :]
            dn = (((1,), (1,)), ((), ()))
            ea = jnp.exp2(lax.dot_general(q, ka, dn, preferred_element_type=jnp.float32) + off)
            eb = jnp.exp2(lax.dot_general(q, kb, dn, preferred_element_type=jnp.float32) + off)
            if masked:
                row = lax.broadcasted_iota(jnp.int32, (NQ, KP), 0) + b * NQ
                col = lax.broadcasted_iota(jnp.int32, (NQ, KP), 1) * 2 + k * KS
                ea = jnp.where(col < row, ea, 0.0)
                eb = jnp.where(col + 1 < row, eb, 0.0)
            ta = 1.0 + ea
            l = jnp.log2(ta * (1.0 + eb)).astype(jnp.bfloat16)
            eb = eb * ta
            s = jnp.dot(l, tri_ref[...], preferred_element_type=jnp.float32)
            g = jnp.exp2(s)
            wa = (ea * g).astype(jnp.bfloat16)
            wb = (eb * g).astype(jnp.bfloat16)
            part = jnp.dot(wa, va_ref[pl.ds(start, KP), :], preferred_element_type=jnp.float32)
            part += jnp.dot(wb, vb_ref[pl.ds(start, KP), :], preferred_element_type=jnp.float32)
            carry = carry_ref[...]
            acc_ref[...] += part * jnp.exp2(carry)
            carry_ref[...] = carry + jnp.broadcast_to(s[:, 0:1], (NQ, 128))
        lax.fori_loop(0, n_hi - n_lo, lambda t, c: (step(n_hi - 1 - t, True), c)[1], 0)
        lax.fori_loop(0, n_lo, lambda t, c: (step(n_lo - 1 - t, False), c)[1], 0)
        o_ref[i] = acc_ref[...].astype(o_ref.dtype)

def attention(q, off, ka, kb, va, vb, blocks_of):
    tri = -jnp.tril(jnp.ones((KP, KP), jnp.bfloat16))
    vm = pl.BlockSpec(memory_space=pltpu.VMEM)
    return pl.pallas_call(
        functools.partial(attention_kernel, blocks_of),
        out_shape=jax.ShapeDtypeStruct(q.shape, jnp.bfloat16),
        in_specs=[vm, pl.BlockSpec(memory_space=pltpu.SMEM)] + [vm] * 5,
        out_specs=vm,
        scratch_shapes=[pltpu.VMEM((NQ, 128), jnp.float32), pltpu.VMEM((NQ, 128), jnp.float32)],
        compiler_params=pltpu.CompilerParams(vmem_limit_bytes=50 * 2**20),
    )(q, off, ka, kb, va, vb, tri)


def rms_rows(inputs, gain_vec):
    inputs = inputs.astype(jnp.float32)
    scaled = inputs * lax.rsqrt(jnp.mean(inputs * inputs, axis=-1, keepdims=True) + NORM_EPS)
    return scaled * gain_vec


def own_blocks():
    group = lax.axis_index("sp_1") * 2 + lax.axis_index("sp_2")
    return [group + 8 * k for k in range(4)]


def on_device(tokens, norm_gain, query_weight, key_weight, value_weight, gate_weight, query_gain, key_gain, score_offset, out_gain, out_weight):
    normed = rms_rows(tokens, norm_gain).astype(jnp.bfloat16)
    rows = lax.all_gather(normed, "tp", axis=0, tiled=True)

    def project(matrix):
        return jnp.dot(rows, matrix, preferred_element_type=jnp.float32).astype(jnp.bfloat16)

    def heads(x):
        return x.reshape(NQ, 4, 128)

    queries = rms_rows(heads(project(query_weight)), query_gain * (LOG2E * 128**-0.5)).astype(jnp.bfloat16)
    keys = rms_rows(heads(project(key_weight)), key_gain).astype(jnp.bfloat16)
    values = heads(project(value_weight))
    gates = project(gate_weight)
    keys, values = (x.reshape(NQ // 2, 2, 4, 128).transpose(2, 1, 0, 3).reshape(4, NQ, 128) for x in (keys, values))
    packed = jnp.stack([queries.transpose(1, 0, 2), keys, values], axis=1)
    packed = lax.all_to_all(packed, "sp_0", split_axis=0, concat_axis=0, tiled=True)
    queries = packed[:, 0]
    both = lax.all_gather(packed[:, 1:], ("sp_1", "sp_2"))
    both = both.reshape(8, 4, 2, 2, NQ // 2, 128).transpose(2, 3, 1, 0, 4, 5).reshape(2, 2, 6144, 128)
    offset = (lax.dynamic_slice_in_dim(score_offset, lax.axis_index("sp_0"), 1) * LOG2E).astype(jnp.float32)
    attended = attention(queries, offset, both[0, 0], both[0, 1], both[1, 0], both[1, 1], own_blocks)
    attended = lax.all_to_all(attended, "sp_0", split_axis=0, concat_axis=0, tiled=True)
    attended = attended.transpose(1, 0, 2)
    normed_out = rms_rows(attended, out_gain.reshape(4, 128)).reshape(NQ, 512)
    mixed = (normed_out * jax.nn.silu(gates.astype(jnp.float32))).astype(jnp.bfloat16)
    partial = jnp.dot(mixed, out_weight, preferred_element_type=jnp.float32).astype(jnp.bfloat16)
    arrived = lax.all_to_all(partial.reshape(4, 96, 4096), "tp", split_axis=0, concat_axis=0, tiled=True)
    return arrived.astype(jnp.float32).sum(axis=0).astype(jnp.bfloat16)


def solution(mesh):
    finer = Mesh(mesh.devices.reshape(4, 4, 2, mesh.shape["tp"]), ("sp_0", "sp_1", "sp_2", "tp"))
    in_specs = (P(SP_TP, None), P(), P(None, "tp"), P(None, "tp"), P(None, "tp"), P(None, "tp"), P(), P(), P("tp"), P("tp"), P("tp", None))
    return jax.shard_map(on_device, mesh=finer, in_specs=in_specs, out_specs=P(SP_TP, None), check_vma=False)
```

time: 1270 us -> 254 us (0.20)
  the two profiles are of different devices: /device:TPU:1 before, /device:TPU:24 now
where the time goes in v1:
time: 254 us
  waiting for transfers between devices  77.6 us (31%)
  blocking collectives  73.8 us (29%)
  Pallas kernels  46.5 us (18%)
  matrix products  24.4 us (10%)
  between operations  14.3 us (6%)
  local copies, waits for them, and re-layouts  9.98 us (4%)
  other arithmetic  7.03 us (3%)
    pallas_call x1, Pallas kernels, attention(): pl.pallas_call(functools.partial(attention_kernel, blocks_of), out_shape=...  46.5 us
    all_gather x1, waiting for transfers between devices, on_device(): rows = lax.all_gather(normed, 'tp', axis=0, tiled=True)  41.6 us
    all_to_all x1, blocking collectives, on_device(): lax.all_to_all(partial.reshape(4, 96, 4096), 'tp', split_axis=0, concat_a...  40.7 us
    all_gather x1, waiting for transfers between devices, on_device(): both = lax.all_gather(packed[:, 1:], ('sp_1', 'sp_2'))  36 us
    all_to_all x1, blocking collectives, on_device(): lax.all_to_all(packed, 'sp_0', split_axis=0, concat_axis=0, tiled=True)  20.6 us
    dot_general x3, matrix products, project(): jnp.dot(rows, matrix, preferred_element_type=jnp.float32)  14.8 us
    all_to_all x1, blocking collectives, on_device(): lax.all_to_all(attended, 'sp_0', split_axis=0, concat_axis=0, tiled=True)  12.6 us
    dot_general x1, matrix products, on_device(): jnp.dot(mixed, out_weight, preferred_element_type=jnp.float32)  9.61 us
  transfers between devices with their start and end apart: 2, of which 2 were waited for; matrix products, arithmetic and copies ran while one was open for 0% of the time, Pallas kernels for 0%

profile of v1, /device:TPU:24, one launch (start us, length us, event | category | flops | bytes accessed | tf_op | source)
XLA Modules:
  0.0 253.6 jit_solution(11731548472774040989)
XLA Ops:
  6.5 0.0 copy-start.2
  6.5 0.0 all-gather.4.cloned.1.call-start
  6.5 1.4 fusion
  8.0 2.3 fusion.2
  10.2 0.0 all-gather.4.cloned.1.call-update
  10.3 0.0 all-gather.6.cloned.1.call-start
  10.3 0.0 copy-done.2
  10.3 41.6 %all-gather.4.cloned.1.call-done = bf16[384,4096]{1,0:T(8,128)(2,1)} async-done(((bf16[96,4096]{1,0:T(8,128)(2,1)}), bf16[384,4096]{1,0:T(8,128)(2,1)}) %all-gather.4.cloned.1.call-update) | async-done | bytes 3145744 | tf_op jit(solution)/shard_map/all_gather | solution.py:84
  52.0 4.9 %convolution_convert_fusion.2 = bf16[384,512]{1,0:T(8,128)(2,1)S(1)} fusion(bf16[384,4096]{1,0:T(8,128)(2,1)} %all-gather.4.cloned.1.call-done, bf16[4096,512]{1,0:T(8,128)(2,1)} %param.15), kind=kOutput, calls=%fused_computation.12 | convolution fusion | flops 1610809344 | bytes 7733248 | tf_op jit(solution)/shard_map/dot_general | solution.py:87
  56.9 0.1 reshape_reshape.3
  57.0 0.1 copy.52
  57.1 0.2 copy.54
  57.3 4.9 %fusion.15 = (f32[384,512]{1,0:T(8,128)S(1)}, f32[384,512]{1,0:T(8,128)S(1)}) fusion(bf16[384,4096]{1,0:T(8,128)(2,1)} %all-gather.4.cloned.1.call-done, bf16[4096,512]{1,0:T(8,128)(2,1)} %param.14), kind=kOutput, calls=%fused_computation.40 | convolution fusion | flops 1611202560 | bytes 8912896 | tf_op jit(solution)/shard_map/dot_general | solution.py:87
  62.2 0.0 copy-start.1
  62.2 0.3 reshape.71
  62.5 0.3 mul.112
  62.8 0.5 reduce_sum.50
  63.3 0.1 copy.50
  63.5 0.0 copy-done.1
  63.5 0.3 fusion.9
  63.7 0.2 copy.53
  64.0 4.9 %fusion.5 = f32[384,512]{1,0:T(8,128)S(1)} fusion(bf16[384,4096]{1,0:T(8,128)(2,1)} %all-gather.4.cloned.1.call-done, bf16[4096,512]{1,0:T(8,128)(2,1)} %param.13), kind=kOutput, calls=%fused_computation.16 | convolution fusion | flops 1611005952 | bytes 8126464 | tf_op jit(solution)/shard_map/dot_general | solution.py:87
  68.9 0.3 copy.47
  69.2 0.1 multiply_reduce_fusion
  69.3 0.1 fusion.10
  69.4 0.2 pad_maximum_fusion
  69.6 0.0 copy-start.3
  69.6 0.8 copy.55
  70.4 20.6 %all_to_all.15 = bf16[4,3,384,128]{3,2,1,0:T(8,128)(2,1)S(1)} all-to-all(bf16[4,3,384,128]{3,2,1,0:T(8,128)(2,1)S(1)} %copy.55), channel_id=1, replica_groups=mesh['sp_0'=4,'sp_1'=4,'sp_2'=2,'tp'=4] {'sp_0'}, dimensions={0} | all-to-all | bytes 2359296 | tf_op jit(solution)/shard_map/all_to_all | solution.py:98
  91.0 0.9 slice.25
  91.9 0.0 all-gather.6.cloned.1.call-update
  91.9 0.0 copy-done.3
  92.0 0.6 dynamic_slice.3
  93.3 36.0 %all-gather.6.cloned.1.call-done = bf16[32,2,384,128]{3,2,1,0:T(8,128)(2,1)} async-done(((bf16[4,2,384,128]{3,2,1,0:T(8,128)(2,1)}), bf16[32,2,384,128]{3,2,1,0:T(8,128)(2,1)}) %all-gather.6.cloned.1.call-update) | async-done | bytes 6291472 | tf_op jit(solution)/shard_map/all_gather | solution.py:100
  129.3 3.4 %copy.57 = bf16[8,4,2,2,192,128]{5,4,0,1,3,2:T(8,128)(2,1)S(1)} copy(bf16[8,4,2,2,192,128]{5,4,3,2,1,0:T(8,128)(2,1)} %bitcast.50) | data formatting | bytes 12582912 | tf_op jit(solution)/shard_map/reshape | solution.py:101
  132.7 2.1 slice_bitcast_fusion
  134.7 0.0 copy-start
  134.7 46.5 %shard_map.109 = bf16[4,384,128]{2,1,0:T(8,128)(2,1)S(1)} custom-call(bf16[4,384,128]{2,1,0:T(8,128)(2,1)S(1)} %slice_bitcast_fusion.4.q_ref, f32[1]{0:T(128)S(6)} %mul.117.off_ref, bf16[6144,128]{1,0:T(8,128)(2,1)S(1)} %get-tuple-element.8.ka_ref, bf16[6144,128]{1,0:T(8,128)(2,1)S(1)} %get-tuple-element.7.kb_ref, ...), custom_call_target="tpu_custom_call" | custom-call | tf_op jit(solution)/shard_map/pallas_call | solution.py:61
  181.2 12.6 %all_to_all.16 = bf16[4,384,128]{2,1,0:T(8,128)(2,1)S(1)} all-to-all(bf16[4,384,128]{2,1,0:T(8,128)(2,1)S(1)} %shard_map.109), channel_id=1, replica_groups=mesh['sp_0'=4,'sp_1'=4,'sp_2'=2,'tp'=4] {'sp_0'}, dimensions={0} | all-to-all | bytes 786432 | tf_op jit(solution)/shard_map/all_to_all | solution.py:104
  193.8 0.3 fusion.6
  194.1 0.0 copy-done
  194.1 0.3 fusion.7
  194.4 0.3 copy.58
  194.7 0.3 copy.59
  194.9 9.6 %convolution_convert_fusion = bf16[384,4096]{1,0:T(8,128)(2,1)} fusion(bf16[512,4096]{1,0:T(8,128)(2,1)} %param.21, f32[384,512]{1,0:T(8,128)S(1)} %copy.59, bf16[384,4096]{1,0:T(8,128)(2,1)} %all-gather.4.cloned.1.call-done, bf16[4096,512]{1,0:T(8,128)(2,1)} %param.16), kind=kOutput, calls=%fused_computation | convolution fusion | flops 3224371200 | bytes 15466496 | tf_op jit(solution)/shard_map/dot_general | solution.py:108
  204.5 40.7 %all_to_all.17 = bf16[4,96,4096]{2,1,0:T(8,128)(2,1)S(1)} all-to-all(bf16[4,96,4096]{2,1,0:T(8,128)(2,1)} %bitcast.51), channel_id=1, replica_groups=mesh['sp_0'=4,'sp_1'=4,'sp_2'=2,'tp'=4] {'tp'}, dimensions={0} | all-to-all | bytes 6291456 | tf_op jit(solution)/shard_map/all_to_all | solution.py:109
  245.2 1.6 reduce_sum.52
  (7 shorter events, 0.1 us)
Async XLA Ops:
  6.5 3.8 %copy-start.2 = (f32[128]{0:T(128)S(1)}, f32[128]{0:T(128)}, u32[]{:S(2)}) copy-start(f32[128]{0:T(128)} %param.17) | copy-start | bytes 1540
  6.5 45.4 %all-gather.4.cloned.1.call-start = ((), (), s32[]{:S(2)}) async-start(), calls=%async_computation.3 | async-start | bytes 3932160 | tf_op jit(solution)/shard_map/all_gather | solution.py:84
  10.3 119.0 %all-gather.6.cloned.1.call-start = ((), (), s32[]{:S(2)}) async-start(), calls=%async_computation.4 | async-start | bytes 7077888 | tf_op jit(solution)/shard_map/all_gather | solution.py:100
  62.2 1.2 copy-start.1
  69.6 22.4 %copy-start.3 = (f32[4]{0:T(128)S(1)}, f32[4]{0:T(128)}, u32[]{:S(2)}) copy-start(f32[4]{0:T(128)} %param.19) | copy-start | bytes 52
  134.7 59.4 %copy-start = (f32[512]{0:T(512)S(1)}, f32[512]{0:T(512)}, u32[]{:S(2)}) copy-start(f32[512]{0:T(512)} %param.20) | copy-start | bytes 6148
Sparse Core Ops, SparseCore 0:
  10.4 41.5 all-gather.3
  92.1 37.1 all-gather.5

commit v2 on v1

v2 whole, which is shorter than its diff:
```python
import functools

import jax
import jax.numpy as jnp
from jax import lax
from jax.experimental import pallas as pl
from jax.experimental.pallas import tpu as pltpu
from jax.sharding import Mesh
from jax.sharding import PartitionSpec as P

SP = ("sp_0", "sp_1", "sp_2")
SP_TP = ("sp_0", "sp_1", "sp_2", "tp")
NORM_EPS = 1e-06

NQ = 384
KS = 512
KP = 256
LOG2E = 1.4426950408889634

def attention_kernel(blocks_of, q_ref, off_ref, kv_ref, tri_ref, o_ref, acc_ref, carry_ref):
    off = off_ref[0]
    blks = blocks_of()
    for i in range(4):
        b = blks[i]
        acc_ref[...] = jnp.zeros_like(acc_ref)
        carry_ref[...] = jnp.zeros_like(carry_ref)
        n_hi = (b * NQ + NQ + KS - 1) // KS
        n_lo = (b * NQ) // KS
        def step(k, masked, i=i, b=b):
            start = pl.multiple_of(k * KP, KP)
            q = q_ref[i]
            ka = kv_ref[0, pl.ds(start, KP), :]
            kb = kv_ref[1, pl.ds(start, KP), :]
            dn = (((1,), (1,)), ((), ()))
            ea = jnp.exp2(lax.dot_general(q, ka, dn, preferred_element_type=jnp.float32) + off)
            eb = jnp.exp2(lax.dot_general(q, kb, dn, preferred_element_type=jnp.float32) + off)
            if masked:
                row = lax.broadcasted_iota(jnp.int32, (NQ, KP), 0) + b * NQ
                col = lax.broadcasted_iota(jnp.int32, (NQ, KP), 1) * 2 + k * KS
                ea = jnp.where(col < row, ea, 0.0)
                eb = jnp.where(col + 1 < row, eb, 0.0)
            ta = 1.0 + ea
            l = jnp.log2(ta * (1.0 + eb)).astype(jnp.bfloat16)
            eb = eb * ta
            s = jnp.dot(l, tri_ref[...], preferred_element_type=jnp.float32)
            g = jnp.exp2(s)
            wa = (ea * g).astype(jnp.bfloat16)
            wb = (eb * g).astype(jnp.bfloat16)
            part = jnp.dot(wa, kv_ref[2, pl.ds(start, KP), :], preferred_element_type=jnp.float32)
            part += jnp.dot(wb, kv_ref[3, pl.ds(start, KP), :], preferred_element_type=jnp.float32)
            carry = carry_ref[...]
            acc_ref[...] += part * jnp.exp2(carry)
            carry_ref[...] = carry + jnp.broadcast_to(s[:, 0:1], (NQ, 128))
        lax.fori_loop(0, n_hi - n_lo, lambda t, c: (step(n_hi - 1 - t, True), c)[1], 0)
        lax.fori_loop(0, n_lo, lambda t, c: (step(n_lo - 1 - t, False), c)[1], 0)
        o_ref[i] = acc_ref[...].astype(o_ref.dtype)

def attention(q, off, kv, blocks_of):
    tri = -jnp.tril(jnp.ones((KP, KP), jnp.bfloat16))
    vm = pl.BlockSpec(memory_space=pltpu.VMEM)
    return pl.pallas_call(
        functools.partial(attention_kernel, blocks_of),
        out_shape=jax.ShapeDtypeStruct(q.shape, jnp.bfloat16),
        in_specs=[vm, pl.BlockSpec(memory_space=pltpu.SMEM)] + [vm] * 2,
        out_specs=vm,
        scratch_shapes=[pltpu.VMEM((NQ, 128), jnp.float32), pltpu.VMEM((NQ, 128), jnp.float32)],
        compiler_params=pltpu.CompilerParams(vmem_limit_bytes=50 * 2**20),
    )(q, off, kv, tri)


MESH = pl.DeviceIdType.MESH
X, Y, Z, C = "tp", "sp_1", "sp_0", "sp_2"
BATCHES = (
    ((0, 0), (0, 1), (0, 2)),
    ((1, 0), (1, 1), (2, 2)),
    ((1, 2), (2, 0), (2, 1)),
    ((3, 0), (3, 1), (3, 2)),
)


def pieces_in_runs(batch):
    runs = []
    for at, (slot, piece) in enumerate(batch):
        if runs and runs[-1][0] == slot and runs[-1][1] + runs[-1][3] == piece:
            runs[-1][3] += 1
        else:
            runs.append([slot, piece, at, 1])
    return runs


RUNS = [pieces_in_runs(batch) for batch in BATCHES]


def projection_kernel(tokens_ref, norm_gain_ref, query_gain_ref, key_gain_ref, wq_ref, wk_ref, wv_ref, wg_ref,
                      kv_ref, q_ref, gate_ref,
                      xbuf, nbuf, wbuf, skv, sq, local_sem, xs, xr, zs, zr, ys, yr, qs, qr):
    x, y, z, c = (lax.axis_index(name) for name in (X, Y, Z, C))
    weight_copies = []
    for kind, ref in enumerate((wk_ref, wv_ref, wq_ref, wg_ref)):
        for half in range(2):
            weight_copies.append(pltpu.make_async_copy(ref.at[:, pl.ds(256 * half, 256)], wbuf.at[2 * kind + half], local_sem.at[2 * kind + half]))
    token_copy = pltpu.make_async_copy(tokens_ref, xbuf.at[0], local_sem.at[8])
    token_copy.start()
    for copy in weight_copies:
        copy.start()
    right, left = {X: lax.rem(x + 1, 4)}, {X: lax.rem(x + 3, 4)}
    up, down = {Y: lax.rem(y + 1, 4)}, {Y: lax.rem(y + 3, 4)}
    sibling = {C: 1 - c}
    barrier = pltpu.get_barrier_semaphore()
    partners = [right, left, up, down, sibling]
    partners += [{Z: lax.rem(z + d, 4)} for d in range(1, 4)]
    partners += [{Z: lax.rem(z + d, 4), Y: 3 - y, C: 1 - c} for d in range(4)]
    for partner in partners:
        pl.semaphore_signal(barrier, inc=1, device_id=partner, device_id_type=MESH)
    pl.semaphore_wait(barrier, len(partners))
    token_copy.wait()

    def remote(src, dst, send, recv, target):
        return pltpu.make_async_remote_copy(src_ref=src, dst_ref=dst, send_sem=send, recv_sem=recv, device_id=target, device_id_type=MESH)

    def piece(slot, p):
        return xbuf.at[slot, pl.ds(32 * p, 32), :]

    to_right = [remote(piece(0, p), piece(1, p), xs.at[p], xr.at[p], right) for p in range(3)]
    to_left = [remote(piece(0, p), piece(2, p), xs.at[3 + p], xr.at[3 + p], left) for p in range(3)]
    for k in range(3):
        to_right[k].start()
        to_left[2 - k].start()
    far = [
        remote(piece(1, 0), piece(3, 0), xs.at[6], xr.at[6], right),
        remote(piece(1 + c, 1), piece(3, 1), xs.at[7], xr.at[7], {X: lax.rem(x + 1 + 2 * c, 4)}),
        remote(piece(2, 2), piece(3, 2), xs.at[8], xr.at[8], left),
    ]

    first = lax.broadcasted_iota(jnp.int32, (96, 96), 0)
    second = lax.broadcasted_iota(jnp.int32, (96, 96), 1)
    shuffle = jnp.where(second == jnp.where(first < 48, 2 * first, 2 * first - 95), 1.0, 0.0).astype(jnp.bfloat16)

    def place(slot):
        return lax.rem(x + (0, 3, 1, 2)[slot], 4)

    def norm_batch(batch):
        gain = norm_gain_ref[...]
        for at, (slot, p) in enumerate(batch):
            for half in range(2):
                rows = xbuf[slot, 32 * p + 16 * half : 32 * p + 16 * half + 16, :].astype(jnp.float32)
                scale = lax.rsqrt(jnp.mean(rows * rows, axis=-1, keepdims=True) + NORM_EPS)
                nbuf[32 * at + 16 * half : 32 * at + 16 * half + 16, :] = (rows * scale * gain).astype(jnp.bfloat16)

    def product(n):
        return jnp.dot(nbuf[...], wbuf[n], preferred_element_type=jnp.float32).astype(jnp.bfloat16)

    def head_norm(rows, gain_ref):
        rows = rows.astype(jnp.float32)
        return (rows * lax.rsqrt(jnp.mean(rows * rows, axis=-1, keepdims=True) + NORM_EPS) * gain_ref[...]).astype(jnp.bfloat16)

    def wait_weights(bt, n):
        if bt == 0:
            weight_copies[n].wait()

    def keys_and_values(bt):
        for half in range(2):
            for kind in range(2):
                wait_weights(bt, 2 * kind + half)
                rows = product(2 * kind + half)
                for i in range(2):
                    part = rows[:, 128 * i : 128 * i + 128]
                    if kind == 0:
                        part = head_norm(part, key_gain_ref)
                    part = jnp.dot(shuffle, part, preferred_element_type=jnp.float32).astype(jnp.bfloat16)
                    skv[bt, 2 * half + i, 2 * kind] = part[:48]
                    skv[bt, 2 * half + i, 2 * kind + 1] = part[48:]

    def queries_and_gates(bt):
        for half in range(2):
            wait_weights(bt, 4 + half)
            rows = product(4 + half)
            for i in range(2):
                sq[bt, 2 * half + i] = head_norm(rows[:, 128 * i : 128 * i + 128], query_gain_ref)
        for half in range(2):
            wait_weights(bt, 6 + half)
            rows = product(6 + half)
            for slot, p, at, count in RUNS[bt]:
                start = pl.multiple_of(96 * place(slot) + 32 * p, 32)
                gate_ref[pl.ds(start, 32 * count), 256 * half : 256 * half + 256] = rows[32 * at : 32 * (at + count)]

    mine = 2 * y + c
    group = {d: 2 * lax.rem(y + d, 4) + c for d in range(4)}
    run_of, runs = {}, []
    for bt in range(4):
        for run in RUNS[bt]:
            run_of.setdefault(bt, []).append(len(runs))
            runs.append((bt, *run))

    def window(r):
        bt, slot, p, at, count = runs[r]
        return pl.ds(pl.multiple_of(48 * place(slot) + 16 * p, 16), 16 * count)

    def query_window(r):
        bt, slot, p, at, count = runs[r]
        return pl.ds(pl.multiple_of(96 * place(slot) + 32 * p, 32), 32 * count)

    def block(r, d):
        return kv_ref.at[:, :, group[d], window(r), :]

    z_copies, up_copies, down_copies, far_copies, side_copies, q_copies = {}, {}, {}, {}, {}, {}
    zig_y = jnp.where(lax.rem(z, 2) == 1, 3 - y, y)
    zig_c = jnp.where(lax.rem(z, 2) == 1, 1 - c, c)
    for r, (bt, slot, p, at, count) in enumerate(runs):
        for d in range(1, 4):
            h = lax.rem(z + d, 4)
            z_copies[r, d] = remote(skv.at[bt, h, :, pl.ds(16 * at, 16 * count), :], kv_ref.at[:, z, mine, window(r), :], zs.at[r, d], zr.at[r, d], {Z: h})
        for d in range(4):
            h = lax.rem(z + d, 4)
            target = {Z: h, Y: zig_y, C: zig_c} if d else {Y: 3 - y, C: 1 - c}
            q_copies[r, d] = remote(sq.at[bt, h, pl.ds(32 * at, 32 * count), :], q_ref.at[z, query_window(r), :], qs.at[r, d], qr.at[r, d], target)
        up_copies[r] = remote(block(r, 0), block(r, 0), ys.at[r, 0], yr.at[r, 0], up)
        down_copies[r] = remote(block(r, 0), block(r, 0), ys.at[r, 1], yr.at[r, 1], down)
        near = kv_ref.at[:, :, 2 * lax.rem(y + 3 + 2 * c, 4) + c, window(r), :]
        far_copies[r] = remote(near, near, ys.at[r, 2], yr.at[r, 2], {Y: lax.rem(y + 1 + 2 * c, 4)})
        for d in range(4):
            side_copies[r, d] = remote(block(r, d), block(r, d), ys.at[r, 3 + d], yr.at[r, 3 + d], sibling)

    def send_z(bt):
        for r in run_of[bt]:
            for d in (2, 1, 3):
                z_copies[r, d].start()
            at, count = runs[r][3], runs[r][4]
            for kind in range(4):
                kv_ref[kind, z, mine, window(r), :] = skv[bt, z, kind, 16 * at : 16 * (at + count), :]

    def send_q(bt):
        for r in run_of[bt]:
            at, count = runs[r][3], runs[r][4]
            for d in range(1, 4):
                q_copies[r, d].start()

            @pl.when(lax.rem(z, 2) == 1)
            def _():
                q_copies[r, 0].start()

            @pl.when(lax.rem(z, 2) == 0)
            def _():
                q_ref[z, query_window(r), :] = sq[bt, z, 32 * at : 32 * (at + count), :]

    def send_y(bt):
        for r in run_of[bt]:
            for d in range(1, 4):
                z_copies[r, d].wait_recv()
            up_copies[r].start()
            down_copies[r].start()
            side_copies[r, 0].start()

    def send_far(bt):
        for r in run_of[bt]:
            up_copies[r].wait_recv()
            down_copies[r].wait_recv()
            far_copies[r].start()
            side_copies[r, 1].start()
            side_copies[r, 3].start()

    def send_last(bt):
        for r in run_of[bt]:
            far_copies[r].wait_recv()
            side_copies[r, 2].start()

    norm_batch(BATCHES[0])
    keys_and_values(0)
    send_z(0)
    queries_and_gates(0)
    send_q(0)
    to_right[0].wait_recv()
    far[0].start()
    to_left[2].wait_recv()
    far[2].start()
    to_right[1].wait_recv()
    to_left[1].wait_recv()
    far[1].start()
    norm_batch(BATCHES[1])
    send_y(0)
    keys_and_values(1)
    send_z(1)
    queries_and_gates(1)
    send_q(1)
    to_right[2].wait_recv()
    to_left[0].wait_recv()
    norm_batch(BATCHES[2])
    send_y(1)
    send_far(0)
    keys_and_values(2)
    send_z(2)
    queries_and_gates(2)
    send_q(2)
    for copy in far:
        copy.wait_recv()
    norm_batch(BATCHES[3])
    send_y(2)
    send_far(1)
    keys_and_values(3)
    send_z(3)
    send_last(0)
    queries_and_gates(3)
    send_q(3)
    send_far(2)
    send_y(3)
    send_last(1)
    send_far(3)
    send_last(2)
    send_last(3)
    for r in range(len(runs)):
        for d in range(4):
            side_copies[r, d].wait_recv()
        for d in range(1, 4):
            q_copies[r, d].wait_recv()

        @pl.when(lax.rem(z, 2) == 1)
        def _():
            q_copies[r, 0].wait_recv()
            q_copies[r, 0].wait_send()

        for d in range(1, 4):
            z_copies[r, d].wait_send()
            q_copies[r, d].wait_send()
        for d in range(4):
            side_copies[r, d].wait_send()
        up_copies[r].wait_send()
        down_copies[r].wait_send()
        far_copies[r].wait_send()
    for copy in to_right + to_left + far:
        copy.wait_send()


def projections(tokens, norm_gain, query_gain, key_gain, wq, wk, wv, wg):
    vm = pl.BlockSpec(memory_space=pltpu.VMEM)
    hbm = pl.BlockSpec(memory_space=pl.ANY)
    count = sum(len(run) for run in RUNS)
    sems = pltpu.SemaphoreType.DMA
    return pl.pallas_call(
        projection_kernel,
        out_shape=(
            jax.ShapeDtypeStruct((4, 4, 8, 192, 128), jnp.bfloat16),
            jax.ShapeDtypeStruct((4, NQ, 128), jnp.bfloat16),
            jax.ShapeDtypeStruct((NQ, 512), jnp.bfloat16),
        ),
        in_specs=[hbm, vm, vm, vm, hbm, hbm, hbm, hbm],
        out_specs=(vm, vm, vm),
        scratch_shapes=[
            pltpu.VMEM((4, 96, 4096), jnp.bfloat16),
            pltpu.VMEM((96, 4096), jnp.bfloat16),
            pltpu.VMEM((8, 4096, 256), jnp.bfloat16),
            pltpu.VMEM((4, 4, 4, 48, 128), jnp.bfloat16),
            pltpu.VMEM((4, 4, 96, 128), jnp.bfloat16),
            sems((9,)), sems((9,)), sems((9,)),
            sems((count, 4)), sems((count, 4)),
            sems((count, 7)), sems((count, 7)),
            sems((count, 4)), sems((count, 4)),
        ],
        compiler_params=pltpu.CompilerParams(collective_id=0, has_side_effects=True, vmem_limit_bytes=48 * 2**20),
    )(tokens, norm_gain.reshape(1, -1), (query_gain * (LOG2E * 128**-0.5)).reshape(1, -1), key_gain.reshape(1, -1), wq, wk, wv, wg)


def rms_rows(inputs, gain_vec):
    inputs = inputs.astype(jnp.float32)
    scaled = inputs * lax.rsqrt(jnp.mean(inputs * inputs, axis=-1, keepdims=True) + NORM_EPS)
    return scaled * gain_vec


def own_blocks():
    group = lax.axis_index("sp_1") * 2 + lax.axis_index("sp_2")
    return [group, 15 - group, 16 + group, 31 - group]


def on_device(tokens, norm_gain, query_weight, key_weight, value_weight, gate_weight, query_gain, key_gain, score_offset, out_gain, out_weight):
    kv, queries, gates = projections(tokens, norm_gain, query_gain, key_gain, query_weight, key_weight, value_weight, gate_weight)
    both = kv.reshape(4, 6144, 128)
    offset = (lax.dynamic_slice_in_dim(score_offset, lax.axis_index("sp_0"), 1) * LOG2E).astype(jnp.float32)
    attended = attention(queries, offset, both, own_blocks)
    turn = [(k, 7 - k) for k in range(8)]
    swapped = lax.ppermute(attended[1::2], ("sp_1", "sp_2"), turn)
    attended = jnp.stack([attended[0], swapped[0], attended[2], swapped[1]])
    attended = lax.all_to_all(attended, "sp_0", split_axis=0, concat_axis=0, tiled=True)
    attended = attended.transpose(1, 0, 2)
    normed_out = rms_rows(attended, out_gain.reshape(4, 128)).reshape(NQ, 512)
    mixed = (normed_out * jax.nn.silu(gates.astype(jnp.float32))).astype(jnp.bfloat16)
    partial = jnp.dot(mixed, out_weight, preferred_element_type=jnp.float32).astype(jnp.bfloat16)
    arrived = lax.all_to_all(partial.reshape(4, 96, 4096), "tp", split_axis=0, concat_axis=0, tiled=True)
    return arrived.astype(jnp.float32).sum(axis=0).astype(jnp.bfloat16)


def solution(mesh):
    finer = Mesh(mesh.devices.reshape(4, 4, 2, mesh.shape["tp"]), ("sp_0", "sp_1", "sp_2", "tp"))
    in_specs = (P(SP_TP, None), P(), P(None, "tp"), P(None, "tp"), P(None, "tp"), P(None, "tp"), P(), P(), P("tp"), P("tp"), P("tp", None))
    return jax.shard_map(on_device, mesh=finer, in_specs=in_specs, out_specs=P(SP_TP, None), check_vma=False)
```

time: 254 us -> 177 us (0.70)
  the two profiles are of different devices: /device:TPU:24 before, /device:TPU:1 now
where the time goes in v2:
time: 177 us
  Pallas kernels  105 us (59%)
  blocking collectives  51 us (29%)
  local copies, waits for them, and re-layouts  6.5 us (4%)
  waiting for transfers between devices  6.27 us (4%)
  matrix products  4.06 us (2%)
  other arithmetic  2.9 us (2%)
    pallas_call x1, Pallas kernels, projections(): pl.pallas_call(projection_kernel, out_shape=(jax.ShapeDtypeStruct((4, 4,...  63.9 us
    pallas_call x1, Pallas kernels, attention(): pl.pallas_call(functools.partial(attention_kernel, blocks_of), out_shape=...  41.3 us
    all_to_all x1, blocking collectives, on_device(): lax.all_to_all(partial.reshape(4, 96, 4096), 'tp', split_axis=0, concat_a...  39.9 us
    all_to_all x1, blocking collectives, on_device(): lax.all_to_all(attended, 'sp_0', split_axis=0, concat_axis=0, tiled=True)  11.1 us
    ppermute x1, waiting for transfers between devices, on_device(): swapped = lax.ppermute(attended[1::2], ('sp_1', 'sp_2'), turn)  6.27 us
    unnamed x10, local copies, waits for them, and re-layouts  4.69 us
    dot_general x1, matrix products, on_device(): jnp.dot(mixed, out_weight, preferred_element_type=jnp.float32)  4.06 us
  transfers between devices with their start and end apart: 1, of which 1 were waited for; matrix products, arithmetic and copies ran while one was open for 0% of the time, Pallas kernels for 0%

profile of v2, /device:TPU:1, one launch (start us, length us, event | category | flops | bytes accessed | tf_op | source)
XLA Modules:
  0.0 176.8 jit_solution(2923908885317592018)
XLA Ops:
  0.0 0.7 multiply_bitcast_fusion.query_gain_ref
  0.7 1.2 dynamic_slice.3
  2.6 0.0 copy-start
  2.6 2.2 %copy-done = bf16[4096,512]{1,0:T(8,128)(2,1)S(1)} copy-done((bf16[4096,512]{1,0:T(8,128)(2,1)S(1)}, bf16[4096,512]{1,0:T(8,128)(2,1)}, u32[]{:S(2)}) %copy-start) | copy-done | bytes 4194328
  4.8 0.0 copy-start.1
  4.8 1.1 copy-done.1
  5.9 0.0 copy-start.2
  5.9 0.7 copy-done.2
  6.6 0.0 copy-start.3
  6.6 0.7 copy-done.3
  7.3 63.9 %shard_map.109 = (bf16[4,4,8,192,128]{4,3,2,1,0:T(8,128)(2,1)}, bf16[4,384,128]{2,1,0:T(8,128)(2,1)S(1)}, bf16[384,512]{1,0:T(8,128)(2,1)S(1)}) custom-call(bf16[96,4096]{1,0:T(8,128)(2,1)S(1)} %copy-done.1, f32[1,4096]{1,0:T(1,128)S(1)} %bitcast.16, f32[1,128]{1,0:T(1,128)S(1)} %multiply_bitcast_fusion.query_gain_ref, f32[1,128]{1,0:T(1,128)S(1)} %bitcast.17, ...), custom_call_target="tpu_custom_call" | custom-call | tf_op jit(solution)/shard_map/pallas_call | solution.py:338
  71.2 0.0 copy-start.4
  71.2 41.3 %shard_map.110 = bf16[4,384,128]{2,1,0:T(8,128)(2,1)S(1)} custom-call(bf16[4,384,128]{2,1,0:T(8,128)(2,1)S(1)} %get-tuple-element.8.q_ref, f32[1]{0:T(128)S(6)} %mul.39.off_ref, bf16[4,6144,128]{2,1,0:T(8,128)(2,1)} %bitcast.18, bf16[256,256]{1,0:T(8,128)(2,1)S(1)} %fusion.10.tri_ref), custom_call_target="tpu_custom_call" | custom-call | tf_op jit(solution)/shard_map/pallas_call | solution.py:61
  112.5 0.1 collective-permute-start
  112.7 6.3 %collective-permute-done = bf16[2,384,128]{2,1,0:T(8,128)(2,1)S(1)} collective-permute-done((bf16[2,384,128]{2,1,0:T(8,128)(2,1)S(1)}, bf16[2,384,128]{2,1,0:T(8,128)(2,1)S(1)}, u32[]{:S(2)}, u32[]{:S(2)}) %collective-permute-start) | collective-permute-done | bytes 196640 | tf_op jit(solution)/shard_map/ppermute | solution.py:379
  119.0 0.1 pad_maximum_fusion
  119.0 11.1 %all_to_all.10 = bf16[4,384,128]{2,1,0:T(8,128)(2,1)S(1)} all-to-all(bf16[4,384,128]{2,1,0:T(8,128)(2,1)S(1)} %pad_maximum_fusion), channel_id=1, replica_groups=mesh['sp_0'=4,'sp_1'=4,'sp_2'=2,'tp'=4] {'sp_0'}, dimensions={0} | all-to-all | bytes 786432 | tf_op jit(solution)/shard_map/all_to_all | solution.py:381
  130.1 0.3 fusion.4
  130.4 0.0 copy-done.4
  130.4 0.3 fusion.5
  130.7 0.3 copy.12
  131.0 0.3 copy.13
  131.2 4.1 %convolution_convert_fusion = bf16[384,4096]{1,0:T(8,128)(2,1)S(1)} fusion(bf16[512,4096]{1,0:T(8,128)(2,1)} %param.21, f32[384,512]{1,0:T(8,128)S(1)} %copy.13, bf16[384,512]{1,0:T(8,128)(2,1)S(1)} %get-tuple-element.10), kind=kOutput, calls=%fused_computation | convolution fusion | flops 1613561856 | bytes 8519680 | tf_op jit(solution)/shard_map/dot_general | solution.py:385
  135.3 39.9 %all_to_all.11 = bf16[4,96,4096]{2,1,0:T(8,128)(2,1)S(1)} all-to-all(bf16[4,96,4096]{2,1,0:T(8,128)(2,1)S(1)} %bitcast.19), channel_id=1, replica_groups=mesh['sp_0'=4,'sp_1'=4,'sp_2'=2,'tp'=4] {'tp'}, dimensions={0} | all-to-all | bytes 6291456 | tf_op jit(solution)/shard_map/all_to_all | solution.py:386
  175.2 1.6 reduce_sum.22
  (5 shorter events, 0.1 us)
Async XLA Ops:
  2.6 2.2 %copy-start = (bf16[4096,512]{1,0:T(8,128)(2,1)S(1)}, bf16[4096,512]{1,0:T(8,128)(2,1)}, u32[]{:S(2)}) copy-start(bf16[4096,512]{1,0:T(8,128)(2,1)} %wq_ref.1) | copy-start | bytes 12582916
  4.8 1.1 copy-start.1
  5.9 0.7 copy-start.2
  6.6 0.7 copy-start.3
  71.2 59.2 %copy-start.4 = (f32[512]{0:T(512)S(1)}, f32[512]{0:T(512)}, u32[]{:S(2)}) copy-start(f32[512]{0:T(512)} %param.20) | copy-start | bytes 6148
  112.5 6.4 %collective-permute-start = (bf16[2,384,128]{2,1,0:T(8,128)(2,1)S(1)}, bf16[2,384,128]{2,1,0:T(8,128)(2,1)S(1)}, u32[]{:S(2)}, u32[]{:S(2)}) collective-permute-start(bf16[2,384,128]{2,1,0:T(8,128)(2,1)S(1)} %slice.16), channel_id=1, source_target_pairs={{0,28},{4,24},{8,20},{12,16},{16,12},{20,8},{24,4},{28,0},{1,29},{... | collective-permute-start | bytes 589832 | tf_op jit(solution)/shard_map/ppermute | solution.py:379

commit v3 on v2

--- a/solution.py
+++ b/solution.py
@@ -8,65 +8,12 @@
 from jax.sharding import Mesh
 from jax.sharding import PartitionSpec as P
 
-SP = ("sp_0", "sp_1", "sp_2")
 SP_TP = ("sp_0", "sp_1", "sp_2", "tp")
 NORM_EPS = 1e-06
-
 NQ = 384
 KS = 512
 KP = 256
 LOG2E = 1.4426950408889634
-
-def attention_kernel(blocks_of, q_ref, off_ref, kv_ref, tri_ref, o_ref, acc_ref, carry_ref):
-    off = off_ref[0]
-    blks = blocks_of()
-    for i in range(4):
-        b = blks[i]
-        acc_ref[...] = jnp.zeros_like(acc_ref)
-        carry_ref[...] = jnp.zeros_like(carry_ref)
-        n_hi = (b * NQ + NQ + KS - 1) // KS
-        n_lo = (b * NQ) // KS
-        def step(k, masked, i=i, b=b):
-            start = pl.multiple_of(k * KP, KP)
-            q = q_ref[i]
-            ka = kv_ref[0, pl.ds(start, KP), :]
-            kb = kv_ref[1, pl.ds(start, KP), :]
-            dn = (((1,), (1,)), ((), ()))
-            ea = jnp.exp2(lax.dot_general(q, ka, dn, preferred_element_type=jnp.float32) + off)
-            eb = jnp.exp2(lax.dot_general(q, kb, dn, preferred_element_type=jnp.float32) + off)
-            if masked:
-                row = lax.broadcasted_iota(jnp.int32, (NQ, KP), 0) + b * NQ
-                col = lax.broadcasted_iota(jnp.int32, (NQ, KP), 1) * 2 + k * KS
-                ea = jnp.where(col < row, ea, 0.0)
-                eb = jnp.where(col + 1 < row, eb, 0.0)
-            ta = 1.0 + ea
-            l = jnp.log2(ta * (1.0 + eb)).astype(jnp.bfloat16)
-            eb = eb * ta
-            s = jnp.dot(l, tri_ref[...], preferred_element_type=jnp.float32)
-            g = jnp.exp2(s)
-            wa = (ea * g).astype(jnp.bfloat16)
-            wb = (eb * g).astype(jnp.bfloat16)
-            part = jnp.dot(wa, kv_ref[2, pl.ds(start, KP), :], preferred_element_type=jnp.float32)
-            part += jnp.dot(wb, kv_ref[3, pl.ds(start, KP), :], preferred_element_type=jnp.float32)
-            carry = carry_ref[...]
-            acc_ref[...] += part * jnp.exp2(carry)
-            carry_ref[...] = carry + jnp.broadcast_to(s[:, 0:1], (NQ, 128))
-        lax.fori_loop(0, n_hi - n_lo, lambda t, c: (step(n_hi - 1 - t, True), c)[1], 0)
-        lax.fori_loop(0, n_lo, lambda t, c: (step(n_lo - 1 - t, False), c)[1], 0)
-        o_ref[i] = acc_ref[...].astype(o_ref.dtype)
-
-def attention(q, off, kv, blocks_of):
-    tri = -jnp.tril(jnp.ones((KP, KP), jnp.bfloat16))
-    vm = pl.BlockSpec(memory_space=pltpu.VMEM)
-    return pl.pallas_call(
-        functools.partial(attention_kernel, blocks_of),
-        out_shape=jax.ShapeDtypeStruct(q.shape, jnp.bfloat16),
-        in_specs=[vm, pl.BlockSpec(memory_space=pltpu.SMEM)] + [vm] * 2,
-        out_specs=vm,
-        scratch_shapes=[pltpu.VMEM((NQ, 128), jnp.float32), pltpu.VMEM((NQ, 128), jnp.float32)],
-        compiler_params=pltpu.CompilerParams(vmem_limit_bytes=50 * 2**20),
-    )(q, off, kv, tri)
-
 
 MESH = pl.DeviceIdType.MESH
 X, Y, Z, C = "tp", "sp_1", "sp_0", "sp_2"
@@ -91,9 +38,9 @@
 RUNS = [pieces_in_runs(batch) for batch in BATCHES]
 
 
-def projection_kernel(tokens_ref, norm_gain_ref, query_gain_ref, key_gain_ref, wq_ref, wk_ref, wv_ref, wg_ref,
-                      kv_ref, q_ref, gate_ref,
-                      xbuf, nbuf, wbuf, skv, sq, local_sem, xs, xr, zs, zr, ys, yr, qs, qr):
+def projection_kernel(tokens_ref, norm_gain_ref, query_gain_ref, key_gain_ref, wq_ref, wk_ref, wv_ref, wg_ref, wo_ref,
+                      kv_ref, q_ref, gate_ref, slice_ref,
+                      xbuf, nbuf, wbuf, skv, sq, sg, local_sem, xs, xr, zs, zr, ys, yr, qs, qr, gs, gr):
     x, y, z, c = (lax.axis_index(name) for name in (X, Y, Z, C))
     weight_copies = []
     for kind, ref in enumerate((wk_ref, wv_ref, wq_ref, wg_ref)):
@@ -101,6 +48,10 @@
             weight_copies.append(pltpu.make_async_copy(ref.at[:, pl.ds(256 * half, 256)], wbuf.at[2 * kind + half], local_sem.at[2 * kind + half]))
     token_copy = pltpu.make_async_copy(tokens_ref, xbuf.at[0], local_sem.at[8])
     token_copy.start()
+    slice_copy = pltpu.make_async_copy(
+        wo_ref.at[pl.ds(pl.multiple_of(128 * z + 32 * y, 32), 32), pl.ds(pl.multiple_of(2048 * c, 2048), 2048)],
+        slice_ref.at[0], local_sem.at[9])
+    slice_copy.start()
     for copy in weight_copies:
         copy.start()
     right, left = {X: lax.rem(x + 1, 4)}, {X: lax.rem(x + 3, 4)}
@@ -180,9 +131,10 @@
         for half in range(2):
             wait_weights(bt, 6 + half)
             rows = product(6 + half)
-            for slot, p, at, count in RUNS[bt]:
-                start = pl.multiple_of(96 * place(slot) + 32 * p, 32)
-                gate_ref[pl.ds(start, 32 * count), 256 * half : 256 * half + 256] = rows[32 * at : 32 * (at + count)]
+            if bt == 0:
+                gate_ref[0, :, 256 * half : 256 * half + 256] = rows
+            else:
+                sg[bt - 1, :, 256 * half : 256 * half + 256] = rows
 
     mine = 2 * y + c
     group = {d: 2 * lax.rem(y + d, 4) + c for d in range(4)}
@@ -203,7 +155,7 @@
     def block(r, d):
         return kv_ref.at[:, :, group[d], window(r), :]
 
-    z_copies, up_copies, down_copies, far_copies, side_copies, q_copies = {}, {}, {}, {}, {}, {}
+    z_copies, up_copies, down_copies, far_copies, side_copies, q_copies, g_copies = {}, {}, {}, {}, {}, {}, {}
     zig_y = jnp.where(lax.rem(z, 2) == 1, 3 - y, y)
     zig_c = jnp.where(lax.rem(z, 2) == 1, 1 - c, c)
     for r, (bt, slot, p, at, count) in enumerate(runs):
@@ -214,6 +166,9 @@
             h = lax.rem(z + d, 4)
             target = {Z: h, Y: zig_y, C: zig_c} if d else {Y: 3 - y, C: 1 - c}
             q_copies[r, d] = remote(sq.at[bt, h, pl.ds(32 * at, 32 * count), :], q_ref.at[z, query_window(r), :], qs.at[r, d], qr.at[r, d], target)
+        if bt:
+            to_rel = (0, 1, 3, 2)[slot]
+            g_copies[r] = remote(sg.at[bt - 1, pl.ds(32 * at, 32 * count), :], gate_ref.at[to_rel, pl.ds(32 * p, 32 * count), :], gs.at[r], gr.at[r], {X: place(slot)})
         up_copies[r] = remote(block(r, 0), block(r, 0), ys.at[r, 0], yr.at[r, 0], up)
         down_copies[r] = remote(block(r, 0), block(r, 0), ys.at[r, 1], yr.at[r, 1], down)
         near = kv_ref.at[:, :, 2 * lax.rem(y + 3 + 2 * c, 4) + c, window(r), :]
@@ -232,6 +187,8 @@
     def send_q(bt):
         for r in run_of[bt]:
             at, count = runs[r][3], runs[r][4]
+            if bt:
+                g_copies[r].start()
             for d in range(1, 4):
                 q_copies[r, d].start()
 
@@ -276,6 +233,10 @@
     to_right[1].wait_recv()
     to_left[1].wait_recv()
     far[1].start()
+    slice_copy.wait()
+    slice_copies = [remote(slice_ref.at[0], slice_ref.at[(4 - d) % 4], xs.at[8 + d], xr.at[8 + d], {X: lax.rem(x + d, 4)}) for d in range(1, 4)]
+    for copy in slice_copies:
+        copy.start()
     norm_batch(BATCHES[1])
     send_y(0)
     keys_and_values(1)
@@ -326,13 +287,17 @@
         up_copies[r].wait_send()
         down_copies[r].wait_send()
         far_copies[r].wait_send()
+        if runs[r][0]:
+            g_copies[r].wait()
+    for copy in slice_copies:
+        copy.wait()
     for copy in to_right + to_left + far:
         copy.wait_send()
 
 
-def projections(tokens, norm_gain, query_gain, key_gain, wq, wk, wv, wg):
+def projections(tokens, norm_gain, query_gain, key_gain, wq, wk, wv, wg, wo):
     vm = pl.BlockSpec(memory_space=pltpu.VMEM)
-    hbm = pl.BlockSpec(memory_space=pl.ANY)
+    hbm = pl.BlockSpec(memory_space=pltpu.HBM)
     count = sum(len(run) for run in RUNS)
     sems = pltpu.SemaphoreType.DMA
     return pl.pallas_call(
@@ -340,51 +305,236 @@
         out_shape=(
             jax.ShapeDtypeStruct((4, 4, 8, 192, 128), jnp.bfloat16),
             jax.ShapeDtypeStruct((4, NQ, 128), jnp.bfloat16),
-            jax.ShapeDtypeStruct((NQ, 512), jnp.bfloat16),
+            jax.ShapeDtypeStruct((4, 96, 512), jnp.bfloat16),
+            jax.ShapeDtypeStruct((4, 32, 2048), jnp.bfloat16),
         ),
-        in_specs=[hbm, vm, vm, vm, hbm, hbm, hbm, hbm],
-        out_specs=(vm, vm, vm),
+        in_specs=[hbm, vm, vm, vm, hbm, hbm, hbm, hbm, hbm],
+        out_specs=(vm, vm, vm, vm),
         scratch_shapes=[
             pltpu.VMEM((4, 96, 4096), jnp.bfloat16),
             pltpu.VMEM((96, 4096), jnp.bfloat16),
             pltpu.VMEM((8, 4096, 256), jnp.bfloat16),
             pltpu.VMEM((4, 4, 4, 48, 128), jnp.bfloat16),
             pltpu.VMEM((4, 4, 96, 128), jnp.bfloat16),
-            sems((9,)), sems((9,)), sems((9,)),
+            pltpu.VMEM((3, 96, 512), jnp.bfloat16),
+            sems((10,)), sems((12,)), sems((12,)),
             sems((count, 4)), sems((count, 4)),
             sems((count, 7)), sems((count, 7)),
             sems((count, 4)), sems((count, 4)),
+            sems((count,)), sems((count,)),
         ],
         compiler_params=pltpu.CompilerParams(collective_id=0, has_side_effects=True, vmem_limit_bytes=48 * 2**20),
-    )(tokens, norm_gain.reshape(1, -1), (query_gain * (LOG2E * 128**-0.5)).reshape(1, -1), key_gain.reshape(1, -1), wq, wk, wv, wg)
-
-
-def rms_rows(inputs, gain_vec):
-    inputs = inputs.astype(jnp.float32)
-    scaled = inputs * lax.rsqrt(jnp.mean(inputs * inputs, axis=-1, keepdims=True) + NORM_EPS)
-    return scaled * gain_vec
-
-
-def own_blocks():
-    group = lax.axis_index("sp_1") * 2 + lax.axis_index("sp_2")
-    return [group, 15 - group, 16 + group, 31 - group]
+    )(tokens, norm_gain.reshape(1, -1), (query_gain * (LOG2E * 128**-0.5)).reshape(1, -1), key_gain.reshape(1, -1), wq, wk, wv, wg, wo)
+
+
+def attention_kernel(q_ref, kv_ref, gate_ref, slice_ref, gain_ref, off_ref, wo_ref, tri_ref, out_ref,
+                     wbuf, att, sa, mx, so, acc_ref, carry_ref, local_sem, ws, wr, as_, ar, ms, mr):
+    x, y, z, c = (lax.axis_index(name) for name in (X, Y, Z, C))
+    group = 2 * y + c
+    barrier = pltpu.get_barrier_semaphore()
+    sibling = {C: 1 - c}
+    partners = [sibling, {Y: lax.rem(y + 1, 4)}, {Y: lax.rem(y + 3, 4)}]
+    for dz in range(4):
+        for dx in range(4):
+            there = {Z: lax.rem(z + dz, 4), X: lax.rem(x + dx, 4)}
+            if dz or dx:
+                partners.append(there)
+            partners.append({**there, Y: 3 - y, C: 1 - c})
+    for partner in partners:
+        pl.semaphore_signal(barrier, inc=1, device_id=partner, device_id_type=MESH)
+    half_columns = pl.ds(pl.multiple_of(2048 * c, 2048), 2048)
+    own_copies = [
+        pltpu.make_async_copy(wo_ref.at[pl.ds(32 * p, 32), half_columns], wbuf.at[0, p // 4, p % 4], local_sem.at[p])
+        for p in range(16)
+    ]
+    for copy in own_copies:
+        copy.start()
+
+    def remote(src, dst, send, recv, target):
+        return pltpu.make_async_remote_copy(src_ref=src, dst_ref=dst, send_sem=send, recv_sem=recv, device_id=target, device_id_type=MESH)
+
+    others = pl.ds(1, 3)
+    rows_a, rows_b = pl.ds(0, 16), pl.ds(16, 16)
+    along_z = [{Z: lax.rem(z + 1, 4)}, {Z: lax.rem(z + 3, 4)}, {Z: lax.rem(z + 1 + 2 * c, 4)}]
+    along_y = [{Y: lax.rem(y + 1, 4)}, {Y: lax.rem(y + 3, 4)}, {Y: lax.rem(y + 1 + 2 * c, 4)}]
+    passed_z, passed_y = lax.rem(z + 3 + 2 * c, 4), lax.rem(y + 3 + 2 * c, 4)
+    every = pl.ds(0, 4)
+
+    def ring(first_src, here, passed, targets, row):
+        copies = [remote(first_src, here, ws.at[row, k], wr.at[row, k], targets[k]) for k in range(2)]
+        return copies + [remote(passed, passed, ws.at[row, 2], wr.at[row, 2], targets[2])]
+
+    a1 = ring(slice_ref.at[others, rows_a], wbuf.at[others, z, y, rows_a], wbuf.at[others, passed_z, y, rows_a], along_z, 0)
+    b1 = ring(slice_ref.at[others, rows_b], wbuf.at[others, z, y, rows_b], wbuf.at[others, z, passed_y, rows_b], along_y, 1)
+    a2 = ring(wbuf.at[others, every, y, rows_a], wbuf.at[others, every, y, rows_a], wbuf.at[others, every, passed_y, rows_a], along_y, 2)
+    b2 = ring(wbuf.at[others, z, every, rows_b], wbuf.at[others, z, every, rows_b], wbuf.at[others, passed_z, every, rows_b], along_z, 3)
+
+    def weights_begin():
+        pl.semaphore_wait(barrier, len(partners))
+        for copies in (a1, b1):
+            copies[0].start()
+            copies[1].start()
+        wbuf[1:4, z, y] = slice_ref[1:4]
+
+    def weights_pass(first, second):
+        for copies in (first, second):
+            copies[0].wait_recv()
+            copies[1].wait_recv()
+            copies[2].start()
+
+    def weights_turn():
+        for copies in (a1, b1):
+            copies[2].wait_recv()
+        for copies in (a2, b2):
+            copies[0].start()
+            copies[1].start()
+
+    off = off_ref[z] * LOG2E
+
+    def steps(i, b, top, count, masked):
+        def step(t, unused):
+            k = top - t
+            start = pl.multiple_of(k * KP, KP)
+            q = q_ref[i]
+            ka = kv_ref[0, pl.ds(start, KP), :]
+            kb = kv_ref[1, pl.ds(start, KP), :]
+            dn = (((1,), (1,)), ((), ()))
+            ea = jnp.exp2(lax.dot_general(q, ka, dn, preferred_element_type=jnp.float32) + off)
+            eb = jnp.exp2(lax.dot_general(q, kb, dn, preferred_element_type=jnp.float32) + off)
+            if masked:
+                row = lax.broadcasted_iota(jnp.int32, (NQ, KP), 0) + b * NQ
+                col = lax.broadcasted_iota(jnp.int32, (NQ, KP), 1) * 2 + k * KS
+                ea = jnp.where(col < row, ea, 0.0)
+                eb = jnp.where(col + 1 < row, eb, 0.0)
+            ta = 1.0 + ea
+            l = jnp.log2(ta * (1.0 + eb)).astype(jnp.bfloat16)
+            eb = eb * ta
+            s = jnp.dot(l, tri_ref[...], preferred_element_type=jnp.float32)
+            g = jnp.exp2(s)
+            wa = (ea * g).astype(jnp.bfloat16)
+            wb = (eb * g).astype(jnp.bfloat16)
+            part = jnp.dot(wa, kv_ref[2, pl.ds(start, KP), :], preferred_element_type=jnp.float32)
+            part += jnp.dot(wb, kv_ref[3, pl.ds(start, KP), :], preferred_element_type=jnp.float32)
+            carry = carry_ref[...]
+            acc_ref[...] += part * jnp.exp2(carry)
+            carry_ref[...] = carry + jnp.broadcast_to(s[:, 0:1], (NQ, 128))
+            return unused
+
+        lax.fori_loop(0, count, step, 0)
+
+    def sends(i):
+        target = {Y: 3 - y, C: 1 - c} if i % 2 else {}
+        out = []
+        for rel in range(4):
+            there = lax.rem(x + 4 - rel, 4)
+            out.append(remote(sa.at[i, pl.ds(pl.multiple_of(96 * there, 32), 96), :], att.at[rel, z], as_.at[i, rel], ar.at[z, rel], {Z: i, X: there, **target}))
+        return out
+
+    def unless_own(i, rel, work):
+        if rel or i % 2:
+            work()
+        else:
+            pl.when(z != i)(work)
+
+    for i in (3, 2, 1, 0):
+        b = 8 * i + (7 - group if i % 2 else group)
+        acc_ref[...] = jnp.zeros_like(acc_ref)
+        carry_ref[...] = jnp.zeros_like(carry_ref)
+        n_hi = (b * NQ + NQ + KS - 1) // KS
+        n_lo = (b * NQ) // KS
+        steps(i, b, n_hi - 1, n_hi - n_lo, True)
+        if i == 3:
+            weights_begin()
+            steps(i, b, n_lo - 1, 7, False)
+            weights_pass(a1, b1)
+            steps(i, b, n_lo - 8, 4, False)
+            weights_turn()
+            steps(i, b, n_lo - 12, n_lo - 11, False)
+        else:
+            steps(i, b, n_lo - 1, n_lo, False)
+        if i == 2:
+            weights_pass(a2, b2)
+        total = acc_ref[...]
+        scale = lax.rsqrt(jnp.mean(total * total, axis=-1, keepdims=True) + NORM_EPS)
+        sa[i] = (total * scale * gain_ref[z]).astype(jnp.bfloat16)
+        for rel, copy in enumerate(sends(i)):
+            unless_own(i, rel, copy.start)
+        if i % 2 == 0:
+            @pl.when(z == i)
+            def _():
+                att[0, z] = sa[i, pl.ds(pl.multiple_of(96 * x, 32), 96), :]
+
+    to_sibling = [remote(mx.at[0, :, pl.ds(512 * r, 512)], mx.at[1, :, pl.ds(512 * r, 512)], ms.at[r], mr.at[r], sibling) for r in range(4)]
+    for r in range(4):
+        for h in range(4):
+            here = att.at[r, h]
+            unless_own(h, r, remote(here, here, as_.at[h, r], ar.at[h, r], sibling).wait_recv)
+        for h in range(4):
+            gate = gate_ref[r, :, 128 * h : 128 * h + 128].astype(jnp.float32)
+            mixed = att[r, h].astype(jnp.float32) * (gate / (1.0 + jnp.exp(-gate)))
+            mx[0, :, 512 * r + 128 * h : 512 * r + 128 * h + 128] = mixed.astype(jnp.bfloat16)
+        to_sibling[r].start()
+    for copies in (a2, b2):
+        copies[2].wait_recv()
+    for copy in own_copies:
+        copy.wait()
+    for copy in to_sibling:
+        copy.wait_recv()
+    backs = []
+    rows = mx[...].reshape(192, 2048)
+    for n in range(8):
+        total = jnp.zeros((192, 256), jnp.float32)
+        for r in range(4):
+            weight = wbuf[r, :, :, :, 256 * n : 256 * n + 256].reshape(512, 256)
+            total += jnp.dot(rows[:, 512 * r : 512 * r + 512], weight, preferred_element_type=jnp.float32)
+        total = total.astype(jnp.bfloat16)
+        columns = pl.ds(pl.multiple_of(2048 * c + 256 * n, 256), 256)
+        so[n] = total[96:]
+        back = remote(so.at[n], out_ref.at[:, columns], ms.at[4 + n], mr.at[4 + n], sibling)
+        back.start()
+        backs.append(back)
+        out_ref[:, columns] = total[:96]
+    for back in backs:
+        back.wait()
+    for copy in to_sibling:
+        copy.wait_send()
+    for i in range(4):
+        for rel, copy in enumerate(sends(i)):
+            unless_own(i, rel, copy.wait_send)
+    for copies in (a1, b1, a2, b2):
+        for copy in copies:
+            copy.wait_send()
+
+
+def attention(q, kv, gates, slices, offset, gain, wo):
+    tri = -jnp.tril(jnp.ones((KP, KP), jnp.bfloat16))
+    vm = pl.BlockSpec(memory_space=pltpu.VMEM)
+    hbm = pl.BlockSpec(memory_space=pltpu.HBM)
+    smem = pl.BlockSpec(memory_space=pltpu.SMEM)
+    sems = pltpu.SemaphoreType.DMA
+    return pl.pallas_call(
+        attention_kernel,
+        out_shape=jax.ShapeDtypeStruct((96, 4096), jnp.bfloat16),
+        in_specs=[vm, vm, vm, vm, vm, smem, hbm, vm],
+        out_specs=vm,
+        scratch_shapes=[
+            pltpu.VMEM((4, 4, 4, 32, 2048), jnp.bfloat16),
+            pltpu.VMEM((4, 4, 96, 128), jnp.bfloat16),
+            pltpu.VMEM((4, NQ, 128), jnp.bfloat16),
+            pltpu.VMEM((2, 96, 2048), jnp.bfloat16),
+            pltpu.VMEM((8, 96, 256), jnp.bfloat16),
+            pltpu.VMEM((NQ, 128), jnp.float32),
+            pltpu.VMEM((NQ, 128), jnp.float32),
+            sems((16,)), sems((4, 3)), sems((4, 3)),
+            sems((4, 4)), sems((4, 4)), sems((12,)), sems((12,)),
+        ],
+        compiler_params=pltpu.CompilerParams(collective_id=1, has_side_effects=True, vmem_limit_bytes=48 * 2**20),
+    )(q, kv, gates, slices, gain.reshape(4, 1, 128), offset, wo, tri)
 
 
 def on_device(tokens, norm_gain, query_weight, key_weight, value_weight, gate_weight, query_gain, key_gain, score_offset, out_gain, out_weight):
-    kv, queries, gates = projections(tokens, norm_gain, query_gain, key_gain, query_weight, key_weight, value_weight, gate_weight)
-    both = kv.reshape(4, 6144, 128)
-    offset = (lax.dynamic_slice_in_dim(score_offset, lax.axis_index("sp_0"), 1) * LOG2E).astype(jnp.float32)
-    attended = attention(queries, offset, both, own_blocks)
-    turn = [(k, 7 - k) for k in range(8)]
-    swapped = lax.ppermute(attended[1::2], ("sp_1", "sp_2"), turn)
-    attended = jnp.stack([attended[0], swapped[0], attended[2], swapped[1]])
-    attended = lax.all_to_all(attended, "sp_0", split_axis=0, concat_axis=0, tiled=True)
-    attended = attended.transpose(1, 0, 2)
-    normed_out = rms_rows(attended, out_gain.reshape(4, 128)).reshape(NQ, 512)
-    mixed = (normed_out * jax.nn.silu(gates.astype(jnp.float32))).astype(jnp.bfloat16)
-    partial = jnp.dot(mixed, out_weight, preferred_element_type=jnp.float32).astype(jnp.bfloat16)
-    arrived = lax.all_to_all(partial.reshape(4, 96, 4096), "tp", split_axis=0, concat_axis=0, tiled=True)
-    return arrived.astype(jnp.float32).sum(axis=0).astype(jnp.bfloat16)
+    kv, queries, gates, slices = projections(tokens, norm_gain, query_gain, key_gain, query_weight, key_weight, value_weight, gate_weight, out_weight)
+    return attention(queries, kv.reshape(4, 6144, 128), gates, slices, score_offset, out_gain, out_weight)
 
 
 def solution(mesh):

time: 177 us -> 136 us (0.77)
  blocking collectives: 51 us -> 0 us
  Pallas kernels: 105 us -> 131 us
  waiting for transfers between devices: 6.27 us -> 0 us
  matrix products: 4.06 us -> 0 us
  local copies, waits for them, and re-layouts: 6.5 us -> 3.39 us
  other arithmetic: 2.9 us -> 0.68 us
    all_to_all x2 -> x0, blocking collectives: 51 us -> none  [the longest x1 39.9 us: on_device(): lax.all_to_all(partial.reshape(4, 96, 4096), 'tp', split_axis=0, concat_a...]
    pallas_call x1, Pallas kernels: 41.3 us -> 66 us  [attention(): pl.pallas_call(attention_kernel, out_shape=jax.ShapeDtypeStruct((96, 4096...]
    ppermute x1 -> x0, waiting for transfers between devices: 6.27 us -> none  [on_device(): swapped = lax.ppermute(attended[1::2], ('sp_1', 'sp_2'), turn)]
    dot_general x1 -> x0, matrix products: 4.06 us -> none  [on_device(): jnp.dot(mixed, out_weight, preferred_element_type=jnp.float32)]
    reduce_sum x2 -> x0, other arithmetic: 1.88 us -> none  [the longest x1 1.6 us: on_device(): return arrived.astype(jnp.float32).sum(axis=0).astype(jnp.bfloat16)]
    unnamed x10 -> x11, local copies, waits for them, and re-layouts: 4.69 us -> 3.39 us
  transfers between devices with their start and end apart: 1 -> 0, of which waited for: 1 -> 0; matrix products, arithmetic and copies ran while one was open for 0% -> 0% of each run, Pallas kernels for 0% -> 0%
where the time goes in v3:
time: 136 us; the launch traced here: 135 us
  Pallas kernels  131 us (96%)
  local copies, waits for them, and re-layouts  3.39 us (2%)
    pallas_call x1, Pallas kernels, attention(): pl.pallas_call(attention_kernel, out_shape=jax.ShapeDtypeStruct((96, 4096...  66 us
    pallas_call x1, Pallas kernels, projections(): pl.pallas_call(projection_kernel, out_shape=(jax.ShapeDtypeStruct((4, 4,...  65.3 us
    unnamed x11, local copies, waits for them, and re-layouts  3.39 us

profile of v3, /device:TPU:1, one launch (start us, length us, event | category | flops | bytes accessed | tf_op | source)
XLA Modules:
  0.0 135.4 jit_solution(906312410986902686)
XLA Ops:
  0.0 0.7 multiply_bitcast_fusion.query_gain_ref
  0.7 0.0 copy-start
  0.7 1.1 copy-done
  1.8 0.0 copy-start.1
  1.8 0.7 copy-done.1
  2.5 0.0 copy-start.3
  2.5 0.7 copy-done.3
  3.2 0.0 copy-start.2
  3.2 0.0 copy-start.4
  3.2 65.3 %shard_map.109 = (bf16[4,4,8,192,128]{4,3,2,1,0:T(8,128)(2,1)}, bf16[4,384,128]{2,1,0:T(8,128)(2,1)S(1)}, bf16[4,96,512]{2,1,0:T(8,128)(2,1)S(1)}, bf16[4,32,2048]{2,1,0:T(8,128)(2,1)S(1)}) custom-call(bf16[96,4096]{1,0:T(8,128)(2,1)S(1)} %copy-done, f32[1,4096]{1,0:T(1,128)S(1)} %bitcast.6, f32[1,128]{1,0:T(1,128)S(1)} %multiply_bitcast_fusion.query_gain_ref, ...), custom_call_target="tpu_custom_call" | custom-call | tf_op jit(solution)/shard_map/pallas_call | solution.py:303
  68.5 0.0 copy-done.2
  68.5 0.0 copy-done.4
  68.5 66.0 %shard_map.110 = bf16[96,4096]{1,0:T(8,128)(2,1)S(1)} custom-call(bf16[4,384,128]{2,1,0:T(8,128)(2,1)S(1)} %get-tuple-element.9.q_ref, bf16[4,6144,128]{2,1,0:T(8,128)(2,1)} %bitcast.9, bf16[4,96,512]{2,1,0:T(8,128)(2,1)S(1)} %get-tuple-element.11.gate_ref, bf16[4,32,2048]{2,1,0:T(8,128)(2,1)S(1)} %get-tuple-element.12.slice_ref, f32[4,1,128]{2,1,0:T(1,128)S(1)} %bitcast.7, ...), custom_call_target="tpu_custom_call" | custom-call | tf_op jit(solution)/shard_map/pallas_call | solution.py:515
  134.6 0.9 copy.13
  (1 shorter events, 0.0 us)
Async XLA Ops:
  0.7 1.1 copy-start
  1.8 0.7 copy-start.1
  2.5 0.7 copy-start.3
  3.2 65.3 %copy-start.2 = (f32[512]{0:T(512)S(1)}, f32[512]{0:T(512)}, u32[]{:S(2)}) copy-start(f32[512]{0:T(512)} %param.20) | copy-start | bytes 6148
  3.2 65.3 %copy-start.4 = (f32[4]{0:T(128)S(1)}, f32[4]{0:T(128)}, u32[]{:S(2)}) copy-start(f32[4]{0:T(128)} %off_ref.1) | copy-start | bytes 52

commit v4 on v3

v4 whole, which is shorter than its diff:
```python
import functools

import jax
import jax.numpy as jnp
from jax import lax
from jax.experimental import pallas as pl
from jax.experimental.pallas import tpu as pltpu
from jax.sharding import Mesh
from jax.sharding import PartitionSpec as P

SP_TP = ("sp_0", "sp_1", "sp_2", "tp")
NORM_EPS = 1e-06
NQ = 384
KS = 512
KP = 256
LOG2E = 1.4426950408889634

MESH = pl.DeviceIdType.MESH
X, Y, Z, C = "tp", "sp_1", "sp_0", "sp_2"
BATCHES = (
    ((0, 0), (0, 1), (0, 2)),
    ((1, 0), (1, 1), (2, 2)),
    ((1, 2), (2, 0), (2, 1)),
    ((3, 0), (3, 1), (3, 2)),
)


def pieces_in_runs(batch):
    runs = []
    for at, (slot, piece) in enumerate(batch):
        if runs and runs[-1][0] == slot and runs[-1][1] + runs[-1][3] == piece:
            runs[-1][3] += 1
        else:
            runs.append([slot, piece, at, 1])
    return runs


RUNS = [pieces_in_runs(batch) for batch in BATCHES]


def layer_kernel(tokens_ref, norm_gain_ref, query_gain_ref, key_gain_ref, wq_ref, wk_ref, wv_ref, wg_ref, wo_ref,
                      gain_ref, off_ref, tri_ref, out_ref,
                      kv_ref, q_ref, gate_ref, slice_ref, wout, wplane, att, sa, mx, so, acc_ref, carry_ref, lbuf, abuf, bbuf,
                      xbuf, nbuf, wbuf, skv, sq, sg, local_sem, xs, xr, zs, zr, ys, yr, qs, qr, gs, gr,
                      out_sem, ws, wr, as_, ar, ms, mr):
    x, y, z, c = (lax.axis_index(name) for name in (X, Y, Z, C))
    weight_copies = []
    for kind, ref in enumerate((wk_ref, wv_ref, wq_ref, wg_ref)):
        for half in range(2):
            weight_copies.append(pltpu.make_async_copy(ref.at[:, pl.ds(256 * half, 256)], wbuf.at[2 * kind + half], local_sem.at[2 * kind + half]))
    token_copy = pltpu.make_async_copy(tokens_ref, xbuf.at[0], local_sem.at[8])
    token_copy.start()
    half_columns = pl.ds(pl.multiple_of(2048 * c, 2048), 2048)
    slice_copy = pltpu.make_async_copy(
        wo_ref.at[pl.ds(pl.multiple_of(256 + 64 * z + 16 * y, 16), 16), half_columns],
        slice_ref.at[0], local_sem.at[9])
    slice_copy.start()
    for copy in weight_copies:
        copy.start()
    own_copies = [pltpu.make_async_copy(wo_ref.at[pl.ds(0, 256), half_columns], wout.at[0, pl.ds(0, 256), :], out_sem.at[16])]
    own_copies += [
        pltpu.make_async_copy(wo_ref.at[pl.ds(256 + 16 * p, 16), half_columns], wplane.at[0, p // 4, p % 4], out_sem.at[p])
        for p in range(16)
    ]
    for copy in own_copies:
        copy.start()
    right, left = {X: lax.rem(x + 1, 4)}, {X: lax.rem(x + 3, 4)}
    up, down = {Y: lax.rem(y + 1, 4)}, {Y: lax.rem(y + 3, 4)}
    sibling = {C: 1 - c}
    barrier = pltpu.get_barrier_semaphore()
    partners = [right, left, up, down, sibling]
    for dz in range(4):
        for dx in range(4):
            there = {Z: lax.rem(z + dz, 4), X: lax.rem(x + dx, 4)}
            if dz or dx % 2 == 0:
                if dz or dx:
                    partners.append(there)
            partners.append({**there, Y: 3 - y, C: 1 - c})
    for partner in partners:
        pl.semaphore_signal(barrier, inc=1, device_id=partner, device_id_type=MESH)
    pl.semaphore_wait(barrier, len(partners))
    token_copy.wait()

    def remote(src, dst, send, recv, target):
        return pltpu.make_async_remote_copy(src_ref=src, dst_ref=dst, send_sem=send, recv_sem=recv, device_id=target, device_id_type=MESH)

    def piece(slot, p):
        return xbuf.at[slot, pl.ds(32 * p, 32), :]

    to_right = [remote(piece(0, p), piece(1, p), xs.at[p], xr.at[p], right) for p in range(3)]
    to_left = [remote(piece(0, p), piece(2, p), xs.at[3 + p], xr.at[3 + p], left) for p in range(3)]
    for k in range(3):
        to_right[k].start()
        to_left[2 - k].start()
    far = [
        remote(piece(1, 0), piece(3, 0), xs.at[6], xr.at[6], right),
        remote(piece(1 + c, 1), piece(3, 1), xs.at[7], xr.at[7], {X: lax.rem(x + 1 + 2 * c, 4)}),
        remote(piece(2, 2), piece(3, 2), xs.at[8], xr.at[8], left),
    ]

    others = pl.ds(1, 3)
    left_columns, right_columns = pl.ds(0, 1024), pl.ds(1024, 1024)
    along_z = [{Z: lax.rem(z + 1, 4)}, {Z: lax.rem(z + 3, 4)}, {Z: lax.rem(z + 1 + 2 * c, 4)}]
    along_y = [{Y: lax.rem(y + 1, 4)}, {Y: lax.rem(y + 3, 4)}, {Y: lax.rem(y + 1 + 2 * c, 4)}]
    passed_z, passed_y = lax.rem(z + 3 + 2 * c, 4), lax.rem(y + 3 + 2 * c, 4)
    every = pl.ds(0, 4)

    def ring(first_src, here, passed, targets, row):
        copies = [remote(first_src, here, ws.at[row, k], wr.at[row, k], targets[k]) for k in range(2)]
        return copies + [remote(passed, passed, ws.at[row, 2], wr.at[row, 2], targets[2])]

    a1 = ring(slice_ref.at[others, :, left_columns], wplane.at[others, z, y, :, left_columns], wplane.at[others, passed_z, y, :, left_columns], along_z, 0)
    b1 = ring(slice_ref.at[others, :, right_columns], wplane.at[others, z, y, :, right_columns], wplane.at[others, z, passed_y, :, right_columns], along_y, 1)
    a2 = ring(wplane.at[others, every, y, :, left_columns], wplane.at[others, every, y, :, left_columns], wplane.at[others, every, passed_y, :, left_columns], along_y, 2)
    b2 = ring(wplane.at[others, z, every, :, right_columns], wplane.at[others, z, every, :, right_columns], wplane.at[others, passed_z, every, :, right_columns], along_z, 3)

    x_ring = [
        remote(wout.at[0, pl.ds(0, 256), :], wout.at[3, pl.ds(0, 256), :], ws.at[4, 0], wr.at[4, 0], right),
        remote(wout.at[0, pl.ds(0, 256), :], wout.at[1, pl.ds(0, 256), :], ws.at[4, 1], wr.at[4, 1], left),
        remote(wout.at[3 - 2 * c, pl.ds(0, 256), :], wout.at[2, pl.ds(0, 256), :], ws.at[4, 2], wr.at[4, 2], {X: lax.rem(x + 1 + 2 * c, 4)}),
    ]

    first = lax.broadcasted_iota(jnp.int32, (96, 96), 0)
    second = lax.broadcasted_iota(jnp.int32, (96, 96), 1)
    shuffle = jnp.where(second == jnp.where(first < 48, 2 * first, 2 * first - 95), 1.0, 0.0).astype(jnp.bfloat16)

    def place(slot):
        return lax.rem(x + (0, 3, 1, 2)[slot], 4)

    def norm_batch(batch):
        gain = norm_gain_ref[...]
        for at, (slot, p) in enumerate(batch):
            for half in range(2):
                rows = xbuf[slot, 32 * p + 16 * half : 32 * p + 16 * half + 16, :].astype(jnp.float32)
                scale = lax.rsqrt(jnp.mean(rows * rows, axis=-1, keepdims=True) + NORM_EPS)
                nbuf[32 * at + 16 * half : 32 * at + 16 * half + 16, :] = (rows * scale * gain).astype(jnp.bfloat16)

    def product(n):
        return jnp.dot(nbuf[...], wbuf[n], preferred_element_type=jnp.float32).astype(jnp.bfloat16)

    def head_norm(rows, gain_ref, factor=1.0):
        rows = rows.astype(jnp.float32)
        return (rows * lax.rsqrt(jnp.mean(rows * rows, axis=-1, keepdims=True) + NORM_EPS) * (gain_ref[...] * factor)).astype(jnp.bfloat16)

    def wait_weights(bt, n):
        if bt == 0:
            weight_copies[n].wait()

    def keys_and_values(bt):
        for half in range(2):
            for kind in range(2):
                wait_weights(bt, 2 * kind + half)
                rows = product(2 * kind + half)
                for i in range(2):
                    part = rows[:, 128 * i : 128 * i + 128]
                    if kind == 0:
                        part = head_norm(part, key_gain_ref)
                    part = jnp.dot(shuffle, part, preferred_element_type=jnp.float32).astype(jnp.bfloat16)
                    skv[bt, 2 * half + i, 2 * kind] = part[:48]
                    skv[bt, 2 * half + i, 2 * kind + 1] = part[48:]

    def queries_and_gates(bt):
        for half in range(2):
            wait_weights(bt, 4 + half)
            rows = product(4 + half)
            for i in range(2):
                sq[bt, 2 * half + i] = head_norm(rows[:, 128 * i : 128 * i + 128], query_gain_ref, LOG2E * 128**-0.5)
        for half in range(2):
            wait_weights(bt, 6 + half)
            rows = product(6 + half)
            if bt == 0:
                gate_ref[0, :, 256 * half : 256 * half + 256] = rows
            else:
                sg[bt - 1, :, 256 * half : 256 * half + 256] = rows

    mine = 2 * y + c
    group = {d: 2 * lax.rem(y + d, 4) + c for d in range(4)}
    run_of, runs = {}, []
    for bt in range(4):
        for run in RUNS[bt]:
            run_of.setdefault(bt, []).append(len(runs))
            runs.append((bt, *run))

    def window(r):
        bt, slot, p, at, count = runs[r]
        return pl.ds(pl.multiple_of(48 * place(slot) + 16 * p, 16), 16 * count)

    def query_window(r):
        bt, slot, p, at, count = runs[r]
        return pl.ds(pl.multiple_of(96 * place(slot) + 32 * p, 32), 32 * count)

    def block(r, d):
        return kv_ref.at[:, :, group[d], window(r), :]

    z_copies, up_copies, down_copies, far_copies, side_copies, q_copies, g_copies = {}, {}, {}, {}, {}, {}, {}
    zig_y = jnp.where(lax.rem(z, 2) == 1, 3 - y, y)
    zig_c = jnp.where(lax.rem(z, 2) == 1, 1 - c, c)
    for r, (bt, slot, p, at, count) in enumerate(runs):
        for d in range(1, 4):
            h = lax.rem(z + d, 4)
            z_copies[r, d] = remote(skv.at[bt, h, :, pl.ds(16 * at, 16 * count), :], kv_ref.at[:, z, mine, window(r), :], zs.at[r, d], zr.at[r, d], {Z: h})
        for d in range(4):
            h = lax.rem(z + d, 4)
            target = {Z: h, Y: zig_y, C: zig_c} if d else {Y: 3 - y, C: 1 - c}
            q_copies[r, d] = remote(sq.at[bt, h, pl.ds(32 * at, 32 * count), :], q_ref.at[z, query_window(r), :], qs.at[r, d], qr.at[r, d], target)
        if bt:
            to_rel = (0, 1, 3, 2)[slot]
            g_copies[r] = remote(sg.at[bt - 1, pl.ds(32 * at, 32 * count), :], gate_ref.at[to_rel, pl.ds(32 * p, 32 * count), :], gs.at[r], gr.at[r], {X: place(slot)})
        up_copies[r] = remote(block(r, 0), block(r, 0), ys.at[r, 0], yr.at[r, 0], up)
        down_copies[r] = remote(block(r, 0), block(r, 0), ys.at[r, 1], yr.at[r, 1], down)
        near = kv_ref.at[:, :, 2 * lax.rem(y + 3 + 2 * c, 4) + c, window(r), :]
        far_copies[r] = remote(near, near, ys.at[r, 2], yr.at[r, 2], {Y: lax.rem(y + 1 + 2 * c, 4)})
        for d in range(4):
            side_copies[r, d] = remote(block(r, d), block(r, d), ys.at[r, 3 + d], yr.at[r, 3 + d], sibling)

    def send_z(bt):
        for r in run_of[bt]:
            for d in (2, 1, 3):
                z_copies[r, d].start()
            at, count = runs[r][3], runs[r][4]
            for kind in range(4):
                kv_ref[kind, z, mine, window(r), :] = skv[bt, z, kind, 16 * at : 16 * (at + count), :]

    def send_q(bt):
        for r in run_of[bt]:
            at, count = runs[r][3], runs[r][4]
            for d in range(1, 4):
                q_copies[r, d].start()

            @pl.when(lax.rem(z, 2) == 1)
            def _():
                q_copies[r, 0].start()

            @pl.when(lax.rem(z, 2) == 0)
            def _():
                q_ref[z, query_window(r), :] = sq[bt, z, 32 * at : 32 * (at + count), :]

    def send_y(bt):
        for r in run_of[bt]:
            for d in range(1, 4):
                z_copies[r, d].wait_recv()
            up_copies[r].start()
            down_copies[r].start()
            side_copies[r, 0].start()

    def send_far(bt):
        for r in run_of[bt]:
            up_copies[r].wait_recv()
            down_copies[r].wait_recv()
            far_copies[r].start()
            side_copies[r, 1].start()
            side_copies[r, 3].start()

    def send_last(bt):
        for r in run_of[bt]:
            far_copies[r].wait_recv()
            side_copies[r, 2].start()

    norm_batch(BATCHES[0])
    keys_and_values(0)
    send_z(0)
    queries_and_gates(0)
    send_q(0)
    to_right[0].wait_recv()
    far[0].start()
    to_left[2].wait_recv()
    far[2].start()
    send_y(0)
    to_right[1].wait_recv()
    to_left[1].wait_recv()
    far[1].start()
    norm_batch(BATCHES[1])
    keys_and_values(1)
    send_z(1)
    send_far(0)
    queries_and_gates(1)
    send_q(1)
    send_y(1)
    to_right[2].wait_recv()
    to_left[0].wait_recv()
    norm_batch(BATCHES[2])
    keys_and_values(2)
    send_z(2)
    send_far(1)
    send_last(0)
    queries_and_gates(2)
    send_q(2)
    send_y(2)
    for copy in far:
        copy.wait_recv()
    slice_copy.wait()
    slice_copies = [remote(slice_ref.at[0], slice_ref.at[(4 - d) % 4], xs.at[8 + d], xr.at[8 + d], {X: lax.rem(x + d, 4)}) for d in range(1, 4)]
    for copy in slice_copies:
        copy.start()
    norm_batch(BATCHES[3])
    keys_and_values(3)
    send_z(3)
    send_last(1)
    queries_and_gates(3)
    send_q(3)
    for copy in own_copies:
        copy.wait()
    for copy in x_ring[:2]:
        copy.start()
    for r in range(len(runs)):
        if runs[r][0]:
            g_copies[r].start()
    send_far(2)
    send_y(3)
    send_last(2)
    send_far(3)
    send_last(3)
    for r in range(len(runs)):
        for d in range(4):
            side_copies[r, d].wait_recv()
        for d in range(1, 4):
            q_copies[r, d].wait_recv()

        @pl.when(lax.rem(z, 2) == 1)
        def _():
            q_copies[r, 0].wait_recv()

    for copy in slice_copies:
        copy.wait_recv()
    def weights_begin():
        for copies in (a1, b1):
            copies[0].start()
            copies[1].start()
        wplane[1:4, z, y] = slice_ref[1:4]

    def weights_pass(first, second):
        for copies in (first, second):
            copies[0].wait_recv()
            copies[1].wait_recv()
            copies[2].start()

    def weights_turn():
        for copies in (a1, b1):
            copies[2].wait_recv()
        for copies in (a2, b2):
            copies[0].start()
            copies[1].start()
        for copy in x_ring[:2]:
            copy.wait_recv()
        x_ring[2].start()

    off = off_ref[z] * LOG2E
    kv_rows = kv_ref.reshape(4, 6144, 128)

    def keys_of(kind, start):
        return kv_rows[kind, pl.ds(start, KP), :]

    weights_begin()

    dn = (((1,), (1,)), ((), ()))

    def score(i, b, k, slot, masked):
        start = pl.multiple_of(jnp.maximum(k, 0) * KP, KP)
        q = q_ref[i]
        ea = jnp.exp2(lax.dot_general(q, keys_of(0, start), dn, preferred_element_type=jnp.float32) + off)
        eb = jnp.exp2(lax.dot_general(q, keys_of(1, start), dn, preferred_element_type=jnp.float32) + off)
        if masked:
            row = lax.broadcasted_iota(jnp.int32, (NQ, KP), 0) + b * NQ
            col = lax.broadcasted_iota(jnp.int32, (NQ, KP), 1) * 2 + k * KS
            ea = jnp.where((col < row) & (col >= 0), ea, 0.0)
            eb = jnp.where((col + 1 < row) & (col >= 0), eb, 0.0)
        ta = 1.0 + ea
        lbuf[slot] = jnp.log2(ta * (1.0 + eb)).astype(jnp.bfloat16)
        abuf[slot] = ea
        bbuf[slot] = eb * ta

    def gather(k, slot):
        start = pl.multiple_of(jnp.maximum(k, 0) * KP, KP)
        s = jnp.dot(lbuf[slot], tri_ref[...], preferred_element_type=jnp.float32)
        g = jnp.exp2(s)
        wa = (abuf[slot] * g).astype(jnp.bfloat16)
        wb = (bbuf[slot] * g).astype(jnp.bfloat16)
        part = jnp.dot(wa, keys_of(2, start), preferred_element_type=jnp.float32)
        part += jnp.dot(wb, keys_of(3, start), preferred_element_type=jnp.float32)
        carry = carry_ref[...]
        acc_ref[...] += part * jnp.exp2(carry)
        carry_ref[...] = carry + jnp.broadcast_to(s[:, 0:1], (NQ, 128))

    def two_steps(i, b, k, masked):
        score(i, b, k, 0, masked)
        score(i, b, k - 1, 1, masked)
        gather(k, 0)
        gather(k - 1, 1)

    def steps(i, b, top, count):
        def pair(t, unused):
            two_steps(i, b, top - 2 * t, False)
            return unused

        def last(t, unused):
            score(i, b, top - count + 1, 0, False)
            gather(top - count + 1, 0)
            return unused

        lax.fori_loop(0, count // 2, pair, 0)
        lax.fori_loop(0, lax.rem(count, 2), last, 0)

    def sends(i):
        target = {Y: 3 - y, C: 1 - c} if i % 2 else {}
        out = []
        for rel in range(4):
            there = lax.rem(x + 4 - rel, 4)
            out.append(remote(sa.at[i, pl.ds(pl.multiple_of(96 * there, 32), 96), :], att.at[rel, z], as_.at[i, rel], ar.at[z, rel], {Z: i, X: there, **target}))
        return out

    def unless_own(i, rel, work):
        if rel or i % 2:
            work()
        else:
            pl.when(z != i)(work)

    for i in (3, 2, 1, 0):
        b = 8 * i + (7 - mine if i % 2 else mine)
        acc_ref[...] = jnp.zeros_like(acc_ref)
        carry_ref[...] = jnp.zeros_like(carry_ref)
        n_hi = (b * NQ + NQ + KS - 1) // KS
        two_steps(i, b, n_hi - 1, True)
        if i == 3:
            steps(i, b, n_hi - 3, 8)
            weights_pass(a1, b1)
            steps(i, b, n_hi - 11, 4)
            weights_turn()
            steps(i, b, n_hi - 15, n_hi - 14)
        else:
            steps(i, b, n_hi - 3, jnp.maximum(n_hi - 2, 0))
        if i == 2:
            weights_pass(a2, b2)
        total = acc_ref[...]
        scale = lax.rsqrt(jnp.mean(total * total, axis=-1, keepdims=True) + NORM_EPS)
        sa[i] = (total * scale * gain_ref[z]).astype(jnp.bfloat16)
        for rel, copy in enumerate(sends(i)):
            unless_own(i, rel, copy.start)
        if i % 2 == 0:
            @pl.when(z == i)
            def _():
                att[0, z] = sa[i, pl.ds(pl.multiple_of(96 * x, 32), 96), :]

    for r in range(len(runs)):
        if runs[r][0]:
            g_copies[r].wait_recv()
    to_sibling = [remote(mx.at[0, :, pl.ds(512 * r, 512)], mx.at[1, :, pl.ds(512 * r, 512)], ms.at[r], mr.at[r], sibling) for r in range(4)]
    for r in range(4):
        for h in range(4):
            here = att.at[r, h]
            unless_own(h, r, remote(here, here, as_.at[h, r], ar.at[h, r], sibling).wait_recv)
        for h in range(4):
            gate = gate_ref[r, :, 128 * h : 128 * h + 128].astype(jnp.float32)
            mixed = att[r, h].astype(jnp.float32) * (gate / (1.0 + jnp.exp(-gate)))
            mx[0, :, 512 * r + 128 * h : 512 * r + 128 * h + 128] = mixed.astype(jnp.bfloat16)
        to_sibling[r].start()
    for copies in (a2, b2):
        copies[2].wait_recv()
    x_ring[2].wait_recv()
    for copy in to_sibling:
        copy.wait_recv()
    backs = []
    rows = mx[...].reshape(192, 2048)
    for n in range(8):
        total = jnp.zeros((192, 256), jnp.float32)
        for r in range(4):
            near = wout[r, :, 256 * n : 256 * n + 256]
            spread = wplane[r, :, :, :, 256 * n : 256 * n + 256].reshape(256, 256)
            total += jnp.dot(rows[:, 512 * r : 512 * r + 256], near, preferred_element_type=jnp.float32)
            total += jnp.dot(rows[:, 512 * r + 256 : 512 * r + 512], spread, preferred_element_type=jnp.float32)
        total = total.astype(jnp.bfloat16)
        columns = pl.ds(pl.multiple_of(2048 * c + 256 * n, 256), 256)
        so[n] = total[96:]
        back = remote(so.at[n], out_ref.at[:, columns], ms.at[4 + n], mr.at[4 + n], sibling)
        back.start()
        backs.append(back)
        out_ref[:, columns] = total[:96]
    for back in backs:
        back.wait()
    for copy in to_sibling:
        copy.wait_send()
    for i in range(4):
        for rel, copy in enumerate(sends(i)):
            unless_own(i, rel, copy.wait_send)
    for copies in (a1, b1, a2, b2, x_ring):
        for copy in copies:
            copy.wait_send()
    for r in range(len(runs)):
        @pl.when(lax.rem(z, 2) == 1)
        def _():
            q_copies[r, 0].wait_send()

        for d in range(1, 4):
            z_copies[r, d].wait_send()
            q_copies[r, d].wait_send()
        for d in range(4):
            side_copies[r, d].wait_send()
        up_copies[r].wait_send()
        down_copies[r].wait_send()
        far_copies[r].wait_send()
        if runs[r][0]:
            g_copies[r].wait_send()
    for copy in slice_copies + to_right + to_left + far:
        copy.wait_send()


def layer(tokens, norm_gain, query_gain, key_gain, wq, wk, wv, wg, wo, offset, gain):
    tri = -jnp.tril(jnp.ones((KP, KP), jnp.bfloat16))
    vm = pl.BlockSpec(memory_space=pltpu.VMEM)
    hbm = pl.BlockSpec(memory_space=pltpu.HBM)
    smem = pl.BlockSpec(memory_space=pltpu.SMEM)
    count = sum(len(run) for run in RUNS)
    sems = pltpu.SemaphoreType.DMA
    half, full = jnp.bfloat16, jnp.float32
    return pl.pallas_call(
        layer_kernel,
        out_shape=jax.ShapeDtypeStruct((96, 4096), jnp.bfloat16),
        in_specs=[hbm, vm, vm, vm, hbm, hbm, hbm, hbm, hbm, vm, smem, vm],
        out_specs=vm,
        scratch_shapes=[
            pltpu.VMEM((4, 4, 8, 192, 128), half),
            pltpu.VMEM((4, NQ, 128), half),
            pltpu.VMEM((4, 96, 512), half),
            pltpu.VMEM((4, 16, 2048), half),
            pltpu.VMEM((4, 256, 2048), half),
            pltpu.VMEM((4, 4, 4, 16, 2048), half),
            pltpu.VMEM((4, 4, 96, 128), half),
            pltpu.VMEM((4, NQ, 128), half),
            pltpu.VMEM((2, 96, 2048), half),
            pltpu.VMEM((8, 96, 256), half),
            pltpu.VMEM((NQ, 128), full),
            pltpu.VMEM((NQ, 128), full),
            pltpu.VMEM((2, NQ, KP), half),
            pltpu.VMEM((2, NQ, KP), full),
            pltpu.VMEM((2, NQ, KP), full),
            pltpu.VMEM((4, 96, 4096), half),
            pltpu.VMEM((96, 4096), half),
            pltpu.VMEM((8, 4096, 256), half),
            pltpu.VMEM((4, 4, 4, 48, 128), half),
            pltpu.VMEM((4, 4, 96, 128), half),
            pltpu.VMEM((3, 96, 512), half),
            sems((10,)), sems((12,)), sems((12,)),
            sems((count, 4)), sems((count, 4)),
            sems((count, 7)), sems((count, 7)),
            sems((count, 4)), sems((count, 4)),
            sems((count,)), sems((count,)),
            sems((17,)), sems((5, 3)), sems((5, 3)),
            sems((4, 4)), sems((4, 4)), sems((12,)), sems((12,)),
        ],
        compiler_params=pltpu.CompilerParams(collective_id=0, has_side_effects=True, vmem_limit_bytes=62 * 2**20),
    )(tokens, norm_gain.reshape(1, -1), query_gain.reshape(1, -1), key_gain.reshape(1, -1), wq, wk, wv, wg, wo, gain.reshape(4, 1, 128), offset, tri)


def on_device(tokens, norm_gain, query_weight, key_weight, value_weight, gate_weight, query_gain, key_gain, score_offset, out_gain, out_weight):
    return layer(tokens, norm_gain, query_gain, key_gain, query_weight, key_weight, value_weight, gate_weight, out_weight, score_offset, out_gain)


def solution(mesh):
    finer = Mesh(mesh.devices.reshape(4, 4, 2, mesh.shape["tp"]), ("sp_0", "sp_1", "sp_2", "tp"))
    in_specs = (P(SP_TP, None), P(), P(None, "tp"), P(None, "tp"), P(None, "tp"), P(None, "tp"), P(), P(), P("tp"), P("tp"), P("tp", None))
    return jax.shard_map(on_device, mesh=finer, in_specs=in_specs, out_specs=P(SP_TP, None), check_vma=False)
```

time: 136 us -> 110 us (0.81)
  Pallas kernels: 131 us -> 107 us
    pallas_call x2 -> x1, Pallas kernels: 131 us -> 107 us  [layer(): pl.pallas_call(layer_kernel, out_shape=jax.ShapeDtypeStruct((96, 4096), j...]
    unnamed x11 -> x1, local copies, waits for them, and re-layouts: 3.39 us -> 2.06 us
where the time goes in v4:
time: 110 us
  Pallas kernels  107 us (97%)
  local copies, waits for them, and re-layouts  2.06 us (2%)
    pallas_call x1, Pallas kernels, layer(): pl.pallas_call(layer_kernel, out_shape=jax.ShapeDtypeStruct((96, 4096), j...  107 us

profile of v4, /device:TPU:1, one launch (start us, length us, event | category | flops | bytes accessed | tf_op | source)
XLA Modules:
  0.0 110.1 jit_solution(14232586328556918308)
XLA Ops:
  0.0 0.7 fusion.1.tri_ref
  0.7 107.3 %shard_map.109 = bf16[96,4096]{1,0:T(8,128)(2,1)} custom-call(bf16[96,4096]{1,0:T(8,128)(2,1)} %tokens_ref.1, f32[1,4096]{1,0:T(1,128)} %bitcast.4, f32[1,128]{1,0:T(1,128)} %bitcast.6, f32[1,128]{1,0:T(1,128)} %bitcast.7, bf16[4096,512]{1,0:T(8,128)(2,1)} %wq_ref.1, bf16[4096,512]{1,0:T(8,128)(2,1)} %wk_ref.1, bf16[4096,512]{1,0:T(8,128)(2,1)} %wv_ref.1, ...), custom_call_target="tpu_custom_call" | custom-call | tf_op jit(solution)/shard_map/pallas_call | solution.py:514
  108.0 2.1 %copy.13 = bf16[96,4096]{1,0:T(8,128)(2,1)} copy(bf16[96,4096]{1,0:T(8,128)(2,1)} %shard_map.109) | data formatting | bytes 1572864

commit v5 on v4

--- a/solution.py
+++ b/solution.py
@@ -39,47 +39,30 @@
 
 
 def layer_kernel(tokens_ref, norm_gain_ref, query_gain_ref, key_gain_ref, wq_ref, wk_ref, wv_ref, wg_ref, wo_ref,
-                      gain_ref, off_ref, tri_ref, out_ref,
-                      kv_ref, q_ref, gate_ref, slice_ref, wout, wplane, att, sa, mx, so, acc_ref, carry_ref, lbuf, abuf, bbuf,
-                      xbuf, nbuf, wbuf, skv, sq, sg, local_sem, xs, xr, zs, zr, ys, yr, qs, qr, gs, gr,
+                      gain_ref, off_ref, out_ref,
+                      kv_ref, q_ref, gate_ref, slice_ref, wout, wplane, att, sa, mx, so, acc_ref, carry_ref, lbuf, abuf, bbuf, tri_ref,
+                      xbuf, nbuf, wbuf, skv, sq, sg, local_sem, xs, xr, zs, zr, ys, yr, qs, qr, gs, gr, fs, fr,
                       out_sem, ws, wr, as_, ar, ms, mr):
     x, y, z, c = (lax.axis_index(name) for name in (X, Y, Z, C))
-    weight_copies = []
-    for kind, ref in enumerate((wk_ref, wv_ref, wq_ref, wg_ref)):
-        for half in range(2):
-            weight_copies.append(pltpu.make_async_copy(ref.at[:, pl.ds(256 * half, 256)], wbuf.at[2 * kind + half], local_sem.at[2 * kind + half]))
+    half_columns = pl.ds(pl.multiple_of(2048 * c, 2048), 2048)
     token_copy = pltpu.make_async_copy(tokens_ref, xbuf.at[0], local_sem.at[8])
     token_copy.start()
-    half_columns = pl.ds(pl.multiple_of(2048 * c, 2048), 2048)
-    slice_copy = pltpu.make_async_copy(
-        wo_ref.at[pl.ds(pl.multiple_of(256 + 64 * z + 16 * y, 16), 16), half_columns],
-        slice_ref.at[0], local_sem.at[9])
-    slice_copy.start()
-    for copy in weight_copies:
-        copy.start()
-    own_copies = [pltpu.make_async_copy(wo_ref.at[pl.ds(0, 256), half_columns], wout.at[0, pl.ds(0, 256), :], out_sem.at[16])]
-    own_copies += [
-        pltpu.make_async_copy(wo_ref.at[pl.ds(256 + 16 * p, 16), half_columns], wplane.at[0, p // 4, p % 4], out_sem.at[p])
-        for p in range(16)
-    ]
-    for copy in own_copies:
-        copy.start()
     right, left = {X: lax.rem(x + 1, 4)}, {X: lax.rem(x + 3, 4)}
     up, down = {Y: lax.rem(y + 1, 4)}, {Y: lax.rem(y + 3, 4)}
     sibling = {C: 1 - c}
     barrier = pltpu.get_barrier_semaphore()
     partners = [right, left, up, down, sibling]
-    for dz in range(4):
-        for dx in range(4):
-            there = {Z: lax.rem(z + dz, 4), X: lax.rem(x + dx, 4)}
-            if dz or dx % 2 == 0:
-                if dz or dx:
-                    partners.append(there)
-            partners.append({**there, Y: 3 - y, C: 1 - c})
+    partners += [{Z: lax.rem(z + d, 4)} for d in range(1, 4)]
     for partner in partners:
         pl.semaphore_signal(barrier, inc=1, device_id=partner, device_id_type=MESH)
+    token_copy.wait()
+    weight_copies = []
+    for kind, ref in enumerate((wk_ref, wv_ref, wq_ref, wg_ref)):
+        for half in range(2):
+            weight_copies.append(pltpu.make_async_copy(ref.at[:, pl.ds(256 * half, 256)], wbuf.at[2 * kind + half], local_sem.at[2 * kind + half]))
+    for copy in weight_copies:
+        copy.start()
     pl.semaphore_wait(barrier, len(partners))
-    token_copy.wait()
 
     def remote(src, dst, send, recv, target):
         return pltpu.make_async_remote_copy(src_ref=src, dst_ref=dst, send_sem=send, recv_sem=recv, device_id=target, device_id_type=MESH)
@@ -120,6 +103,9 @@
         remote(wout.at[3 - 2 * c, pl.ds(0, 256), :], wout.at[2, pl.ds(0, 256), :], ws.at[4, 2], wr.at[4, 2], {X: lax.rem(x + 1 + 2 * c, 4)}),
     ]
 
+    tri_ref[...] = jnp.where(
+        lax.broadcasted_iota(jnp.int32, (KP, KP), 0) >= lax.broadcasted_iota(jnp.int32, (KP, KP), 1), -1.0, 0.0
+    ).astype(jnp.bfloat16)
     first = lax.broadcasted_iota(jnp.int32, (96, 96), 0)
     second = lax.broadcasted_iota(jnp.int32, (96, 96), 1)
     shuffle = jnp.where(second == jnp.where(first < 48, 2 * first, 2 * first - 95), 1.0, 0.0).astype(jnp.bfloat16)
@@ -127,9 +113,11 @@
     def place(slot):
         return lax.rem(x + (0, 3, 1, 2)[slot], 4)
 
-    def norm_batch(batch):
+    def norm_batch(batch, only=(0, 1, 2)):
         gain = norm_gain_ref[...]
         for at, (slot, p) in enumerate(batch):
+            if at not in only:
+                continue
             for half in range(2):
                 rows = xbuf[slot, 32 * p + 16 * half : 32 * p + 16 * half + 16, :].astype(jnp.float32)
                 scale = lax.rsqrt(jnp.mean(rows * rows, axis=-1, keepdims=True) + NORM_EPS)
@@ -156,15 +144,17 @@
                     if kind == 0:
                         part = head_norm(part, key_gain_ref)
                     part = jnp.dot(shuffle, part, preferred_element_type=jnp.float32).astype(jnp.bfloat16)
-                    skv[bt, 2 * half + i, 2 * kind] = part[:48]
-                    skv[bt, 2 * half + i, 2 * kind + 1] = part[48:]
-
-    def queries_and_gates(bt):
+                    skv[bt, 2 * half + i, :, 256 * kind : 256 * kind + 128] = part[:48]
+                    skv[bt, 2 * half + i, :, 256 * kind + 128 : 256 * kind + 256] = part[48:]
+
+    def queries(bt):
         for half in range(2):
             wait_weights(bt, 4 + half)
             rows = product(4 + half)
             for i in range(2):
                 sq[bt, 2 * half + i] = head_norm(rows[:, 128 * i : 128 * i + 128], query_gain_ref, LOG2E * 128**-0.5)
+
+    def gates(bt):
         for half in range(2):
             wait_weights(bt, 6 + half)
             rows = product(6 + half)
@@ -190,7 +180,7 @@
         return pl.ds(pl.multiple_of(96 * place(slot) + 32 * p, 32), 32 * count)
 
     def block(r, d):
-        return kv_ref.at[:, :, group[d], window(r), :]
+        return kv_ref.at[:, group[d], window(r), :]
 
     z_copies, up_copies, down_copies, far_copies, side_copies, q_copies, g_copies = {}, {}, {}, {}, {}, {}, {}
     zig_y = jnp.where(lax.rem(z, 2) == 1, 3 - y, y)
@@ -198,7 +188,7 @@
     for r, (bt, slot, p, at, count) in enumerate(runs):
         for d in range(1, 4):
             h = lax.rem(z + d, 4)
-            z_copies[r, d] = remote(skv.at[bt, h, :, pl.ds(16 * at, 16 * count), :], kv_ref.at[:, z, mine, window(r), :], zs.at[r, d], zr.at[r, d], {Z: h})
+            z_copies[r, d] = remote(skv.at[bt, h, pl.ds(16 * at, 16 * count), :], kv_ref.at[z, mine, window(r), :], zs.at[r, d], zr.at[r, d], {Z: h})
         for d in range(4):
             h = lax.rem(z + d, 4)
             target = {Z: h, Y: zig_y, C: zig_c} if d else {Y: 3 - y, C: 1 - c}
@@ -206,20 +196,54 @@
         if bt:
             to_rel = (0, 1, 3, 2)[slot]
             g_copies[r] = remote(sg.at[bt - 1, pl.ds(32 * at, 32 * count), :], gate_ref.at[to_rel, pl.ds(32 * p, 32 * count), :], gs.at[r], gr.at[r], {X: place(slot)})
+        if bt == 3:
+            continue
         up_copies[r] = remote(block(r, 0), block(r, 0), ys.at[r, 0], yr.at[r, 0], up)
         down_copies[r] = remote(block(r, 0), block(r, 0), ys.at[r, 1], yr.at[r, 1], down)
-        near = kv_ref.at[:, :, 2 * lax.rem(y + 3 + 2 * c, 4) + c, window(r), :]
+        near = kv_ref.at[:, 2 * lax.rem(y + 3 + 2 * c, 4) + c, window(r), :]
         far_copies[r] = remote(near, near, ys.at[r, 2], yr.at[r, 2], {Y: lax.rem(y + 1 + 2 * c, 4)})
         for d in range(4):
             side_copies[r, d] = remote(block(r, d), block(r, d), ys.at[r, 3 + d], yr.at[r, 3 + d], sibling)
+
+    fine = len(runs) - 1
+    fine_up, fine_down, fine_far, fine_side = {}, {}, {}, {}
+    for d in range(4):
+        source = lax.rem(z + 4 - d, 4)
+
+        def part(place_y):
+            return kv_ref.at[source, place_y, window(fine), :]
+
+        fine_up[d] = remote(part(mine), part(mine), fs.at[d, 0], fr.at[d, 0], up)
+        fine_down[d] = remote(part(mine), part(mine), fs.at[d, 1], fr.at[d, 1], down)
+        near = 2 * lax.rem(y + 3 + 2 * c, 4) + c
+        fine_far[d] = remote(part(near), part(near), fs.at[d, 2], fr.at[d, 2], {Y: lax.rem(y + 1 + 2 * c, 4)})
+        for k in range(4):
+            fine_side[d, k] = remote(part(group[k]), part(group[k]), fs.at[d, 3 + k], fr.at[d, 3 + k], sibling)
+
+    def fine_near(d):
+        if d:
+            z_copies[fine, d].wait_recv()
+        fine_up[d].start()
+        fine_down[d].start()
+        fine_side[d, 0].start()
+
+    def fine_pass(d):
+        fine_up[d].wait_recv()
+        fine_down[d].wait_recv()
+        fine_far[d].start()
+        fine_side[d, 1].start()
+        fine_side[d, 3].start()
+
+    def fine_last(d):
+        fine_far[d].wait_recv()
+        fine_side[d, 2].start()
 
     def send_z(bt):
         for r in run_of[bt]:
             for d in (2, 1, 3):
                 z_copies[r, d].start()
             at, count = runs[r][3], runs[r][4]
-            for kind in range(4):
-                kv_ref[kind, z, mine, window(r), :] = skv[bt, z, kind, 16 * at : 16 * (at + count), :]
+            kv_ref[z, mine, window(r), :] = skv[bt, z, 16 * at : 16 * (at + count), :]
 
     def send_q(bt):
         for r in run_of[bt]:
@@ -256,11 +280,36 @@
             far_copies[r].wait_recv()
             side_copies[r, 2].start()
 
+    def weights_begin():
+        for copies in (a1, b1):
+            copies[0].start()
+            copies[1].start()
+        wplane[1:4, z, y] = slice_ref[1:4]
+
+    def weights_pass(first, second):
+        for copies in (first, second):
+            copies[0].wait_recv()
+            copies[1].wait_recv()
+            copies[2].start()
+
+    def weights_turn():
+        for copies in (a1, b1):
+            copies[2].wait_recv()
+        for copies in (a2, b2):
+            copies[0].start()
+            copies[1].start()
+
+    def weights_pass_x():
+        for copy in x_ring[:2]:
+            copy.wait_recv()
+        x_ring[2].start()
+
+
     norm_batch(BATCHES[0])
     keys_and_values(0)
     send_z(0)
-    queries_and_gates(0)
-    send_q(0)
+    queries(0)
+    gates(0)
     to_right[0].wait_recv()
     far[0].start()
     to_left[2].wait_recv()
@@ -269,12 +318,25 @@
     to_right[1].wait_recv()
     to_left[1].wait_recv()
     far[1].start()
+    own_copies = [pltpu.make_async_copy(wo_ref.at[pl.ds(0, 256), half_columns], wout.at[0, pl.ds(0, 256), :], out_sem.at[16])]
+    own_copies += [
+        pltpu.make_async_copy(wo_ref.at[pl.ds(256 + 16 * p, 16), half_columns], wplane.at[0, p // 4, p % 4], out_sem.at[p])
+        for p in range(16)
+    ]
+    for copy in own_copies:
+        copy.start()
+    slice_copy = pltpu.make_async_copy(
+        wo_ref.at[pl.ds(pl.multiple_of(256 + 64 * z + 16 * y, 16), 16), half_columns],
+        slice_ref.at[0], local_sem.at[9])
+    slice_copy.start()
     norm_batch(BATCHES[1])
     keys_and_values(1)
     send_z(1)
     send_far(0)
-    queries_and_gates(1)
+    send_q(0)
+    queries(1)
     send_q(1)
+    gates(1)
     send_y(1)
     to_right[2].wait_recv()
     to_left[0].wait_recv()
@@ -283,36 +345,48 @@
     send_z(2)
     send_far(1)
     send_last(0)
-    queries_and_gates(2)
+    queries(2)
     send_q(2)
+    gates(2)
     send_y(2)
-    for copy in far:
-        copy.wait_recv()
+    for k in (0, 2, 1):
+        far[k].wait_recv()
+        norm_batch(BATCHES[3], (k,))
     slice_copy.wait()
     slice_copies = [remote(slice_ref.at[0], slice_ref.at[(4 - d) % 4], xs.at[8 + d], xr.at[8 + d], {X: lax.rem(x + d, 4)}) for d in range(1, 4)]
     for copy in slice_copies:
         copy.start()
-    norm_batch(BATCHES[3])
-    keys_and_values(3)
-    send_z(3)
-    send_last(1)
-    queries_and_gates(3)
-    send_q(3)
     for copy in own_copies:
         copy.wait()
     for copy in x_ring[:2]:
         copy.start()
+    keys_and_values(3)
+    send_z(3)
+    fine_near(0)
+    send_last(1)
+    queries(3)
+    send_q(3)
+    fine_near(1)
+    fine_near(3)
+    send_far(2)
+    fine_near(2)
+    fine_pass(0)
+    gates(3)
+    fine_pass(1)
+    fine_pass(3)
+    fine_pass(2)
+    for copy in slice_copies:
+        copy.wait_recv()
+    weights_begin()
+    send_last(2)
+    for d in (0, 1, 3, 2):
+        fine_last(d)
     for r in range(len(runs)):
         if runs[r][0]:
             g_copies[r].start()
-    send_far(2)
-    send_y(3)
-    send_last(2)
-    send_far(3)
-    send_last(3)
     for r in range(len(runs)):
         for d in range(4):
-            side_copies[r, d].wait_recv()
+            (side_copies[r, d] if r != fine else fine_side[d, 0]).wait_recv()
         for d in range(1, 4):
             q_copies[r, d].wait_recv()
 
@@ -320,37 +394,15 @@
         def _():
             q_copies[r, 0].wait_recv()
 
-    for copy in slice_copies:
-        copy.wait_recv()
-    def weights_begin():
-        for copies in (a1, b1):
-            copies[0].start()
-            copies[1].start()
-        wplane[1:4, z, y] = slice_ref[1:4]
-
-    def weights_pass(first, second):
-        for copies in (first, second):
-            copies[0].wait_recv()
-            copies[1].wait_recv()
-            copies[2].start()
-
-    def weights_turn():
-        for copies in (a1, b1):
-            copies[2].wait_recv()
-        for copies in (a2, b2):
-            copies[0].start()
-            copies[1].start()
-        for copy in x_ring[:2]:
-            copy.wait_recv()
-        x_ring[2].start()
-
+    for d in range(4):
+        for k in range(1, 4):
+            fine_side[d, k].wait_recv()
     off = off_ref[z] * LOG2E
-    kv_rows = kv_ref.reshape(4, 6144, 128)
+    kv_rows = kv_ref.reshape(6144, 512)
 
     def keys_of(kind, start):
-        return kv_rows[kind, pl.ds(start, KP), :]
-
-    weights_begin()
+        return kv_rows[pl.ds(start, KP), 128 * kind : 128 * kind + 128]
+
 
     dn = (((1,), (1,)), ((), ()))
 
@@ -421,15 +473,18 @@
         n_hi = (b * NQ + NQ + KS - 1) // KS
         two_steps(i, b, n_hi - 1, True)
         if i == 3:
+            weights_pass(a1, b1)
+            steps(i, b, n_hi - 3, 6)
+            weights_turn()
+            steps(i, b, n_hi - 9, 6)
+            weights_pass_x()
+            steps(i, b, n_hi - 15, n_hi - 14)
+        elif i == 2:
             steps(i, b, n_hi - 3, 8)
-            weights_pass(a1, b1)
-            steps(i, b, n_hi - 11, 4)
-            weights_turn()
-            steps(i, b, n_hi - 15, n_hi - 14)
+            weights_pass(a2, b2)
+            steps(i, b, n_hi - 11, n_hi - 10)
         else:
             steps(i, b, n_hi - 3, jnp.maximum(n_hi - 2, 0))
-        if i == 2:
-            weights_pass(a2, b2)
         total = acc_ref[...]
         scale = lax.rsqrt(jnp.mean(total * total, axis=-1, keepdims=True) + NORM_EPS)
         sa[i] = (total * scale * gain_ref[z]).astype(jnp.bfloat16)
@@ -492,19 +547,22 @@
         for d in range(1, 4):
             z_copies[r, d].wait_send()
             q_copies[r, d].wait_send()
-        for d in range(4):
-            side_copies[r, d].wait_send()
-        up_copies[r].wait_send()
-        down_copies[r].wait_send()
-        far_copies[r].wait_send()
+        if r != fine:
+            for d in range(4):
+                side_copies[r, d].wait_send()
+            up_copies[r].wait_send()
+            down_copies[r].wait_send()
+            far_copies[r].wait_send()
         if runs[r][0]:
             g_copies[r].wait_send()
+    for d in range(4):
+        for copy in (fine_up[d], fine_down[d], fine_far[d], *(fine_side[d, k] for k in range(4))):
+            copy.wait_send()
     for copy in slice_copies + to_right + to_left + far:
         copy.wait_send()
 
 
 def layer(tokens, norm_gain, query_gain, key_gain, wq, wk, wv, wg, wo, offset, gain):
-    tri = -jnp.tril(jnp.ones((KP, KP), jnp.bfloat16))
     vm = pl.BlockSpec(memory_space=pltpu.VMEM)
     hbm = pl.BlockSpec(memory_space=pltpu.HBM)
     smem = pl.BlockSpec(memory_space=pltpu.SMEM)
@@ -514,10 +572,10 @@
     return pl.pallas_call(
         layer_kernel,
         out_shape=jax.ShapeDtypeStruct((96, 4096), jnp.bfloat16),
-        in_specs=[hbm, vm, vm, vm, hbm, hbm, hbm, hbm, hbm, vm, smem, vm],
+        in_specs=[hbm, vm, vm, vm, hbm, hbm, hbm, hbm, hbm, vm, smem],
         out_specs=vm,
         scratch_shapes=[
-            pltpu.VMEM((4, 4, 8, 192, 128), half),
+            pltpu.VMEM((4, 8, 192, 512), half),
             pltpu.VMEM((4, NQ, 128), half),
             pltpu.VMEM((4, 96, 512), half),
             pltpu.VMEM((4, 16, 2048), half),
@@ -532,10 +590,11 @@
             pltpu.VMEM((2, NQ, KP), half),
             pltpu.VMEM((2, NQ, KP), full),
             pltpu.VMEM((2, NQ, KP), full),
+            pltpu.VMEM((KP, KP), half),
             pltpu.VMEM((4, 96, 4096), half),
             pltpu.VMEM((96, 4096), half),
             pltpu.VMEM((8, 4096, 256), half),
-            pltpu.VMEM((4, 4, 4, 48, 128), half),
+            pltpu.VMEM((4, 4, 48, 512), half),
             pltpu.VMEM((4, 4, 96, 128), half),
             pltpu.VMEM((3, 96, 512), half),
             sems((10,)), sems((12,)), sems((12,)),
@@ -543,11 +602,12 @@
             sems((count, 7)), sems((count, 7)),
             sems((count, 4)), sems((count, 4)),
             sems((count,)), sems((count,)),
+            sems((4, 7)), sems((4, 7)),
             sems((17,)), sems((5, 3)), sems((5, 3)),
             sems((4, 4)), sems((4, 4)), sems((12,)), sems((12,)),
         ],
-        compiler_params=pltpu.CompilerParams(collective_id=0, has_side_effects=True, vmem_limit_bytes=62 * 2**20),
-    )(tokens, norm_gain.reshape(1, -1), query_gain.reshape(1, -1), key_gain.reshape(1, -1), wq, wk, wv, wg, wo, gain.reshape(4, 1, 128), offset, tri)
+        compiler_params=pltpu.CompilerParams(collective_id=0, has_side_effects=True, vmem_limit_bytes=56 * 2**20),
+    )(tokens, norm_gain.reshape(1, -1), query_gain.reshape(1, -1), key_gain.reshape(1, -1), wq, wk, wv, wg, wo, gain.reshape(4, 1, 128), offset)
 
 
 def on_device(tokens, norm_gain, query_weight, key_weight, value_weight, gate_weight, query_gain, key_gain, score_offset, out_gain, out_weight):

time: 110 us -> 106 us (0.964)
  Pallas kernels: 107 us -> 104 us
    pallas_call x1, Pallas kernels: 107 us -> 104 us  [layer(): pl.pallas_call(layer_kernel, out_shape=jax.ShapeDtypeStruct((96, 4096), j...]
where the time goes in v5:
time: 106 us
  Pallas kernels  104 us (98%)
  local copies, waits for them, and re-layouts  2.06 us (2%)
    pallas_call x1, Pallas kernels, layer(): pl.pallas_call(layer_kernel, out_shape=jax.ShapeDtypeStruct((96, 4096), j...  104 us

profile of v5, /device:TPU:1, one launch (start us, length us, event | category | flops | bytes accessed | tf_op | source)
XLA Modules:
  0.0 106.1 jit_solution(17779500063073066475)
XLA Ops:
  0.0 104.0 %shard_map.109 = bf16[96,4096]{1,0:T(8,128)(2,1)} custom-call(bf16[96,4096]{1,0:T(8,128)(2,1)} %tokens_ref.1, f32[1,4096]{1,0:T(1,128)} %bitcast.4, f32[1,128]{1,0:T(1,128)} %bitcast.6, f32[1,128]{1,0:T(1,128)} %bitcast.7, bf16[4096,512]{1,0:T(8,128)(2,1)} %wq_ref.1, bf16[4096,512]{1,0:T(8,128)(2,1)} %wk_ref.1, bf16[4096,512]{1,0:T(8,128)(2,1)} %wv_ref.1, ...), custom_call_target="tpu_custom_call" | custom-call | tf_op jit(solution)/shard_map/pallas_call | solution.py:572
  104.0 2.1 %copy.13 = bf16[96,4096]{1,0:T(8,128)(2,1)} copy(bf16[96,4096]{1,0:T(8,128)(2,1)} %shard_map.109) | data formatting | bytes 1572864

commit v6 on v5

--- a/solution.py
+++ b/solution.py
@@ -40,7 +40,7 @@
 
 def layer_kernel(tokens_ref, norm_gain_ref, query_gain_ref, key_gain_ref, wq_ref, wk_ref, wv_ref, wg_ref, wo_ref,
                       gain_ref, off_ref, out_ref,
-                      kv_ref, q_ref, gate_ref, slice_ref, wout, wplane, att, sa, mx, so, acc_ref, carry_ref, lbuf, abuf, bbuf, tri_ref,
+                      kv_ref, q_ref, gate_ref, slice_ref, wout, wplane, att, sa, mx, so, acc_ref, carry_ref, lbuf, fbuf, abuf, bbuf, tri_ref,
                       xbuf, nbuf, wbuf, skv, sq, sg, local_sem, xs, xr, zs, zr, ys, yr, qs, qr, gs, gr, fs, fr,
                       out_sem, ws, wr, as_, ar, ms, mr):
     x, y, z, c = (lax.axis_index(name) for name in (X, Y, Z, C))
@@ -104,7 +104,7 @@
     ]
 
     tri_ref[...] = jnp.where(
-        lax.broadcasted_iota(jnp.int32, (KP, KP), 0) >= lax.broadcasted_iota(jnp.int32, (KP, KP), 1), -1.0, 0.0
+        lax.broadcasted_iota(jnp.int32, (KP, KP), 0) > lax.broadcasted_iota(jnp.int32, (KP, KP), 1), -1.0, 0.0
     ).astype(jnp.bfloat16)
     first = lax.broadcasted_iota(jnp.int32, (96, 96), 0)
     second = lax.broadcasted_iota(jnp.int32, (96, 96), 1)
@@ -417,13 +417,15 @@
             ea = jnp.where((col < row) & (col >= 0), ea, 0.0)
             eb = jnp.where((col + 1 < row) & (col >= 0), eb, 0.0)
         ta = 1.0 + ea
-        lbuf[slot] = jnp.log2(ta * (1.0 + eb)).astype(jnp.bfloat16)
+        logs = jnp.log2(ta * (1.0 + eb))
+        lbuf[slot] = logs.astype(jnp.bfloat16)
+        fbuf[slot] = logs
         abuf[slot] = ea
         bbuf[slot] = eb * ta
 
     def gather(k, slot):
         start = pl.multiple_of(jnp.maximum(k, 0) * KP, KP)
-        s = jnp.dot(lbuf[slot], tri_ref[...], preferred_element_type=jnp.float32)
+        s = jnp.dot(lbuf[slot], tri_ref[...], preferred_element_type=jnp.float32) - fbuf[slot]
         g = jnp.exp2(s)
         wa = (abuf[slot] * g).astype(jnp.bfloat16)
         wb = (bbuf[slot] * g).astype(jnp.bfloat16)
@@ -590,6 +592,7 @@
             pltpu.VMEM((2, NQ, KP), half),
             pltpu.VMEM((2, NQ, KP), full),
             pltpu.VMEM((2, NQ, KP), full),
+            pltpu.VMEM((2, NQ, KP), full),
             pltpu.VMEM((KP, KP), half),
             pltpu.VMEM((4, 96, 4096), half),
             pltpu.VMEM((96, 4096), half),

time: 106 us -> 107 us (level)
  no operation moved by 1% of the time
where the time goes in v6:
time: 107 us; the launch traced here: 106 us
  Pallas kernels  104 us (97%)
  local copies, waits for them, and re-layouts  2.06 us (2%)
    pallas_call x1, Pallas kernels, layer(): pl.pallas_call(layer_kernel, out_shape=jax.ShapeDtypeStruct((96, 4096), j...  104 us

profile of v6, /device:TPU:1, one launch (start us, length us, event | category | flops | bytes accessed | tf_op | source)
XLA Modules:
  0.0 106.4 jit_solution(935699226770380980)
XLA Ops:
  0.0 104.3 %shard_map.109 = bf16[96,4096]{1,0:T(8,128)(2,1)} custom-call(bf16[96,4096]{1,0:T(8,128)(2,1)} %tokens_ref.1, f32[1,4096]{1,0:T(1,128)} %bitcast.4, f32[1,128]{1,0:T(1,128)} %bitcast.6, f32[1,128]{1,0:T(1,128)} %bitcast.7, bf16[4096,512]{1,0:T(8,128)(2,1)} %wq_ref.1, bf16[4096,512]{1,0:T(8,128)(2,1)} %wk_ref.1, bf16[4096,512]{1,0:T(8,128)(2,1)} %wv_ref.1, ...), custom_call_target="tpu_custom_call" | custom-call | tf_op jit(solution)/shard_map/pallas_call | solution.py:574
  104.3 2.1 %copy.13 = bf16[96,4096]{1,0:T(8,128)(2,1)} copy(bf16[96,4096]{1,0:T(8,128)(2,1)} %shard_map.109) | data formatting | bytes 1572864
